TPU v7x, 32 devices: a whole 2x2x4 slice. The times are simulated.
32 devices in a mesh: sp: 4 (over y, core), tp: 8 (over z, x).
Axes of the slice: x: 2, y: 2, z: 4, core: 2. Of those that a mesh axis runs over, the one named last changes fastest.
Arguments:
- queries: bfloat16 [512, 3072], P('sp'), may hold values from -6 to 6
- attn_out: bfloat16 [512, 3072], P('sp'), may hold values from -3 to 3
- log_norm: float32 [512, 12], P('sp'), as said below
- cotangent: bfloat16 [512, 3072], P('sp'), may hold values from -96 to 96
- keys: bfloat16 [1024, 512], P(('sp', 'tp')), may hold values from -6 to 6
- values: bfloat16 [1024, 512], P(('sp', 'tp')), may hold values from -6 to 6
- source: bfloat16 [1024, 3072], P('sp', 'tp'), may hold values from -6 to 6
- w_query: bfloat16 [3072, 3072], P('tp'), may hold values from -0.109375 to 0.109375
- w_key: bfloat16 [3072, 512], P('tp'), may hold values from -0.109375 to 0.109375
- w_value: bfloat16 [3072, 512], P('tp'), may hold values from -0.109375 to 0.109375
Outputs:
- d_target: bfloat16 [512, 3072], P('sp', 'tp')
- d_source: bfloat16 [1024, 3072], P('sp', 'tp')
- d_wvalue: float32 [3072, 512], P('tp')
Inputs may be any that keep to these rules, and one draw needn't show every extreme that they name: `log_norm`: the logarithm of the softmax total saved by the forward pass, near log(1024) + 0.5.
All inputs are finite; a program needn't handle non-finite values.
Results may differ from a plain program's by a relative error of at most 0.024.
Values may be sent and summed in bfloat16 or wider, within the bound.
No kernel may reach another device: no remote copies, remote signals or barrier semaphores. Data moves between devices by JAX's collectives and lax.ppermute only.
A program may use at most 64 MiB of HBM per device.

v0:
```python
import math

import jax
import jax.numpy as jnp
from jax import lax
from jax.sharding import PartitionSpec as P

HEADS = 12
KV_HEADS = 2
HEAD_DIM = 256


def shards(queries, attn_out, log_norm, cotangent, keys, values, source, w_query, w_key, w_value):
    single_precision = jnp.float32
    repeat = HEADS // KV_HEADS
    score_scale = 1.0 / math.sqrt(HEAD_DIM)
    rows = queries.shape[0]
    near_keys, near_values = (
        lax.all_gather(keys, "sp", axis=0, tiled=True),
        lax.all_gather(values, "sp", axis=0, tiled=True),
    )
    span = near_keys.shape[0]
    query_tensor4 = queries.reshape(rows, KV_HEADS, repeat, HEAD_DIM)
    output_gradient4 = cotangent.reshape(rows, KV_HEADS, repeat, HEAD_DIM)
    out4 = attn_out.reshape(rows, KV_HEADS, repeat, HEAD_DIM)
    shared_key_heads = near_keys.reshape(span, KV_HEADS, HEAD_DIM)
    shared_value_heads = near_values.reshape(span, KV_HEADS, HEAD_DIM)
    delta = jnp.sum(
        output_gradient4.astype(single_precision) * out4.astype(single_precision), axis=3
    )
    delta = jnp.transpose(delta, (1, 2, 0))[..., None]
    lse = jnp.transpose(log_norm.reshape(rows, KV_HEADS, repeat), (1, 2, 0))[..., None]
    logit_scores = (
        jnp.einsum(
            "znjk,wnk->njzw",
            query_tensor4,
            shared_key_heads,
            preferred_element_type=single_precision,
        )
        * score_scale
    )
    probs = jnp.exp(logit_scores - lse)
    probabilities16 = probs.astype(jnp.bfloat16)
    prob_gradient = jnp.einsum(
        "znjk,wnk->njzw",
        output_gradient4,
        shared_value_heads,
        preferred_element_type=single_precision,
    )
    score_gradient = (probs * (prob_gradient - delta)).astype(jnp.bfloat16)
    query_gradient_piece = (
        jnp.einsum(
            "wohn,nwb->hwob",
            score_gradient,
            shared_key_heads,
            preferred_element_type=single_precision,
        )
        * score_scale
    )
    query_gradient_piece = query_gradient_piece.reshape(rows, -1)
    key_gradient_piece = (
        jnp.einsum(
            "nkjv,jnka->vna", score_gradient, query_tensor4, preferred_element_type=single_precision
        )
        * score_scale
    )
    value_gradient_piece = jnp.einsum(
        "nkjv,jnka->vna", probabilities16, output_gradient4, preferred_element_type=single_precision
    )
    own_keys, own_values = (
        lax.psum_scatter(
            key_gradient_piece.reshape(span, -1).astype(jnp.bfloat16),
            "sp",
            scatter_dimension=0,
            tiled=True,
        ).astype(jnp.float32),
        lax.psum_scatter(
            value_gradient_piece.reshape(span, -1).astype(jnp.bfloat16),
            "sp",
            scatter_dimension=0,
            tiled=True,
        ).astype(jnp.float32),
    )
    stacked = jnp.concatenate(
        [own_keys.astype(jnp.bfloat16), own_values.astype(jnp.bfloat16)], axis=1
    )
    group = lax.all_gather(stacked, "tp", axis=0, tiled=True)
    weights = jnp.concatenate([w_key, w_value], axis=1)
    d_source = lax.dot_general(
        group, weights, (((1,), (1,)), ((), ())), preferred_element_type=single_precision
    ).astype(jnp.bfloat16)
    kv_width = w_value.shape[1]
    weight_term = lax.dot_general(
        source,
        group[:, kv_width:],
        (((0,), (0,)), ((), ())),
        preferred_element_type=single_precision,
    )
    d_wvalue = lax.psum(weight_term.astype(jnp.bfloat16), "sp").astype(jnp.float32)
    dq16 = lax.psum(query_gradient_piece, "tp").astype(jnp.bfloat16)
    d_target = lax.dot_general(
        dq16, w_query, (((1,), (1,)), ((), ())), preferred_element_type=single_precision
    ).astype(jnp.bfloat16)
    return (d_target, d_source, d_wvalue)


def solution(mesh):
    in_specs = (
        P("sp", None),
        P("sp", None),
        P("sp", None),
        P("sp", None),
        P(("sp", "tp"), None),
        P(("sp", "tp"), None),
        P("sp", "tp"),
        P("tp", None),
        P("tp", None),
        P("tp", None),
    )
    out_specs = (P("sp", "tp"), P("sp", "tp"), P("tp", None))
    return jax.shard_map(shards, mesh=mesh, in_specs=in_specs, out_specs=out_specs, check_vma=False)
```

profile of v0, /device:TPU:0, one launch (start us, length us, event | category | flops | bytes accessed | tf_op | source)
XLA Modules:
  0.0 197.1 jit_solution(18364416684558412824)
XLA Ops:
  7.2 0.0 reduce-scatter.9.cloned.1.call-start
  7.2 0.8 reshape.35
  8.1 6.7 %all_gather.9 = bf16[128,512]{1,0:T(8,128)(2,1)S(1)} all-gather(bf16[32,512]{1,0:T(8,128)(2,1)} %param.14), channel_id=1, replica_groups=mesh['sp'=4,'tp'=8] {'sp'}, dimensions={0}, use_global_device_ids=true | all-gather | bytes 163840 | tf_op jit(solution)/shard_map/all_gather | solution.py:19
  14.8 0.1 copy.36
  14.9 2.3 %copy.37 = bf16[128,3072]{0,1:T(8,128)(2,1)} copy(bf16[128,3072]{1,0:T(8,128)(2,1)} %param.10) | data formatting | bytes 1572864 | tf_op args[0]
  17.3 1.5 copy.41
  18.8 1.5 fusion.4
  20.3 0.9 copy-done.2
  21.2 0.4 fusion.11
  21.5 0.1 copy.51
  21.7 0.8 copy.73
  22.5 0.0 reduce-scatter.7.cloned.1.call-start
  22.5 5.6 %all_gather.10 = bf16[128,512]{1,0:T(8,128)(2,1)S(1)} all-gather(bf16[32,512]{1,0:T(8,128)(2,1)S(1)} %copy-done.8), channel_id=1, replica_groups=mesh['sp'=4,'tp'=8] {'sp'}, dimensions={0}, use_global_device_ids=true | all-gather | bytes 163840 | tf_op jit(solution)/shard_map/all_gather | solution.py:20
  28.1 0.8 copy.40
  28.9 2.3 %copy.44 = bf16[128,3072]{0,1:T(8,128)(2,1)} copy(bf16[128,3072]{1,0:T(8,128)(2,1)} %param.11) | data formatting | bytes 1572864 | tf_op args[1]
  31.2 1.5 fusion
  32.7 0.3 fusion.6
  33.0 0.4 fusion.12
  33.4 0.1 copy.49
  33.5 0.8 copy.71
  34.3 0.0 reduce-scatter.7.cloned.1.call-update
  34.3 0.0 all-reduce.3.cloned.1.call-start
  34.4 1.6 multiply_bitcast_fusion
  36.0 3.0 %copy.47 = f32[128,2,6,256]{0,3,2,1:T(8,128)} copy(f32[128,2,6,256]{3,0,2,1:T(8,128)} %multiply_bitcast_fusion) | data formatting | bytes 3145728 | tf_op jit(solution)/shard_map/mul | solution.py:52
  39.0 80.8 %all-reduce.4 = bf16[128,3072]{0,1:T(8,128)(2,1)S(1)} all-reduce(f32[128,3072]{0,1:T(8,128)} %bitcast.80), channel_id=1, replica_groups=mesh['sp'=4,'tp'=8] {'tp'}, use_global_device_ids=true, to_apply=%region_1.0 | all-reduce | flops 393216 | bytes 2359296 | tf_op jit(solution)/shard_map/psum | solution.py:100
  119.9 1.5 convolution_convert_fusion.2
  121.4 0.8 pad_maximum_fusion
  122.1 31.5 %all_gather.11 = bf16[256,1024]{1,0:T(8,128)(2,1)S(1)} all-gather(bf16[32,1024]{1,0:T(8,128)(2,1)S(1)} %pad_maximum_fusion), channel_id=1, replica_groups=mesh['sp'=4,'tp'=8] {'tp'}, dimensions={0}, use_global_device_ids=true | all-gather | bytes 589824 | tf_op jit(solution)/shard_map/all_gather | solution.py:87
  153.6 1.1 fusion.7
  154.7 2.3 %convolution_convert_fusion.1 = bf16[256,384]{1,0:T(8,128)(2,1)} fusion(bf16[256,1024]{1,0:T(8,128)(2,1)S(1)} %all_gather.11, bf16[384,512]{1,0:T(8,128)(2,1)} %param.19, bf16[384,512]{1,0:T(8,128)(2,1)} %param.18), kind=kOutput, calls=%fused_computation.13 | convolution fusion | flops 202997760 | bytes 1507328 | tf_op jit(solution)/shard_map/dot_general | solution.py:89
  157.0 31.5 %all-reduce.3.cloned.1.call-done = bf16[384,512]{0,1:T(8,128)(2,1)} async-done(((bf16[384,512]{0,1:T(8,128)(2,1)}), bf16[384,512]{0,1:T(8,128)(2,1)}) %all-reduce.3.cloned.1.call-update) | async-done | bytes 393232 | tf_op jit(solution)/shard_map/psum | solution.py:99
  188.5 2.0 %copy.54 = f32[384,512]{1,0:T(8,128)} copy(bf16[384,512]{0,1:T(8,128)(2,1)} %all-reduce.3.cloned.1.call-done) | data formatting | bytes 1179648
  (21 shorter events, 0.1 us)
Async XLA Ops:
  7.2 112.7 %copy-start = (bf16[384,3072]{1,0:T(8,128)(2,1)S(1)}, bf16[384,3072]{1,0:T(8,128)(2,1)}, u32[]{:S(2)}) copy-start(bf16[384,3072]{1,0:T(8,128)(2,1)} %param.17) | copy-start | bytes 7077892
  7.2 114.2 %reduce-scatter.9.cloned.1.call-start = ((), (), s32[]{:S(2)}) async-start(), calls=%async_computation.4 | async-start | bytes 163840 | tf_op jit(solution)/shard_map/reduce_scatter | solution.py:77
  14.9 3.9 %copy-start.4 = (bf16[128,512]{0,1:T(8,128)(2,1)}, bf16[128,512]{0,1:T(8,128)(2,1)S(1)}, u32[]{:S(2)}) copy-start(bf16[128,512]{0,1:T(8,128)(2,1)S(1)} %copy.36) | copy-start | bytes 393220
  20.3 0.9 copy-start.2
  20.3 2.2 %copy-start.8 = (bf16[32,512]{1,0:T(8,128)(2,1)S(1)}, bf16[32,512]{1,0:T(8,128)(2,1)}, u32[]{:S(2)}) copy-start(bf16[32,512]{1,0:T(8,128)(2,1)} %param.15) | copy-start | bytes 98308
  22.5 98.9 %reduce-scatter.7.cloned.1.call-start = ((), (), s32[]{:S(2)}) async-start(), calls=%async_computation.3 | async-start | bytes 163840 | tf_op jit(solution)/shard_map/reduce_scatter | solution.py:71
  31.2 1.5 copy-start.3
  31.2 1.5 copy-start.6
  31.2 1.8 copy-start.1
  33.0 1.4 copy-start.5
  34.3 154.2 %all-reduce.3.cloned.1.call-start = ((), (), s32[]{:S(2)}) async-start(), calls=%async_computation.2 | async-start | bytes 786432 | tf_op jit(solution)/shard_map/psum | solution.py:99
  119.9 33.8 %copy-start.7 = (bf16[256,384]{1,0:T(8,128)(2,1)S(1)}, bf16[256,384]{1,0:T(8,128)(2,1)}, u32[]{:S(2)}) copy-start(bf16[256,384]{1,0:T(8,128)(2,1)} %param.16) | copy-start | bytes 589828
Sparse Core Ops, SparseCore 0:
  22.6 21.2 reduce-scatter.8
  46.9 19.6 reduce-scatter.6
  154.9 33.6 all-reduce.2
where the time goes:
time: 198 us; the launch traced here: 197 us
  blocking collectives  125 us (63%)
  waiting for transfers between devices  31.6 us (16%)
  local copies, waits for them, and re-layouts  15.6 us (8%)
  between operations  13.9 us (7%)
  matrix products  8.94 us (5%)
  other arithmetic  2.26 us (1%)
    psum x1, blocking collectives, shards(): dq16 = lax.psum(query_gradient_piece, 'tp').astype(jnp.bfloat16)  80.8 us
    psum x1, waiting for transfers between devices, shards(): lax.psum(weight_term.astype(jnp.bfloat16), 'sp').astype(jnp.float32)  31.5 us
    all_gather x1, blocking collectives, shards(): group = lax.all_gather(stacked, 'tp', axis=0, tiled=True)  31.5 us
    unnamed x24, local copies, waits for them, and re-layouts  10.6 us
    all_gather x1, blocking collectives, shards(): lax.all_gather(keys, 'sp', axis=0, tiled=True)  6.73 us
    all_gather x1, blocking collectives, shards(): lax.all_gather(values, 'sp', axis=0, tiled=True)  5.59 us
  transfers between devices with their start and end apart: 3, of which 1 were waited for; matrix products, arithmetic and copies ran while one was open for 7% of the time, Pallas kernels for 0%

commit v1 on v0

v1 whole, which is shorter than its diff:
```python
import functools
import math

import jax
import jax.numpy as jnp
from jax import lax
from jax.experimental import pallas as pl
from jax.experimental.pallas import tpu as pltpu
from jax.sharding import PartitionSpec as P

HEADS = 12
KV_HEADS = 2
HEAD_DIM = 256
GROUP = HEADS // KV_HEADS
SCALE = 1.0 / math.sqrt(HEAD_DIM)
F32 = jnp.float32
BF16 = jnp.bfloat16
VMEM = pl.BlockSpec(memory_space=pltpu.VMEM)
SMEM = pl.BlockSpec(memory_space=pltpu.SMEM)


def dot(a, b, contract):
    return lax.dot_general(a, b, (contract, ((), ())), preferred_element_type=F32)


NN = ((1,), (0,))
NT = ((1,), (1,))
TN = ((0,), (0,))


def call(kernel, outs, scratch, flops, operands, specs=None, name=None):
    moved = sum(x.size * x.dtype.itemsize for x in operands)
    moved += sum(math.prod(o.shape) * o.dtype.itemsize for o in outs)
    return pl.pallas_call(
        kernel,
        out_shape=outs,
        in_specs=specs or [VMEM] * len(operands),
        out_specs=[VMEM] * len(outs),
        scratch_shapes=scratch,
        cost_estimate=pl.CostEstimate(flops=flops, bytes_accessed=moved, transcendentals=0),
        compiler_params=pltpu.CompilerParams(vmem_limit_bytes=24 * 1024 * 1024),
        name=name,
    )(*operands)


def prepare_kernel(q_ref, do_ref, o_ref, qs_ref, dos_ref, delta_ref):
    rows = q_ref.shape[0]
    lanes = lax.broadcasted_iota(jnp.int32, (rows, 128), 1)
    columns = jnp.zeros((rows, 128), F32)
    for h in range(HEADS):
        span = slice(h * HEAD_DIM, (h + 1) * HEAD_DIM)
        there = slice(h * rows, (h + 1) * rows)
        qs_ref[there, :] = q_ref[:, span]
        grad = do_ref[:, span]
        dos_ref[there, :] = grad
        total = jnp.sum(grad.astype(F32) * o_ref[:, span].astype(F32), axis=1, keepdims=True)
        columns = jnp.where(lanes == h, total, columns)
    delta_ref[...] = columns.T[: delta_ref.shape[0], :]


def chunk_kernel(tiles, blocks, each, first, last, *refs):
    n_pieces = sum(len(t) for t in tiles)
    refs = list(refs)
    start_ref, half_ref, lse_ref, delta_ref, q_ref, do_ref, wk_ref, wv_ref = refs[:8]
    source = {(0, 0): refs[8], (1, 0): refs[9], (0, 1): refs[10], (1, 1): refs[11]}
    pieces = refs[12 : 12 + n_pieces]
    refs = refs[12 + n_pieces :]
    if not first:
        old_ref = refs.pop(0)
    ds_ref, near_ref, far_ref = refs[:3]
    refs = refs[3:]
    if last:
        wv_near_ref, wv_far_ref = refs[:2]
        refs = refs[2:]
    else:
        total_ref = refs.pop(0)
    if last:
        total_ref = refs.pop()
    p_ref, dkv_ref, src_ref = refs
    width = wk_ref.shape[1]
    rows = q_ref.shape[0] // HEADS
    stacked = GROUP * rows
    step = 2 * rows
    row, index = 0, 0
    near_row, far_row = 0, 0
    fresh = first
    for tile in tiles:
        held = [pieces[i] for i in tile]
        height = sum(x.shape[0] for x in held)
        for g in range(KV_HEADS):
            cols = slice(g * HEAD_DIM, (g + 1) * HEAD_DIM)
            vcols = slice(width + g * HEAD_DIM, width + (g + 1) * HEAD_DIM)
            k = jnp.concatenate([x[:, cols] for x in held], axis=0)
            v = jnp.concatenate([x[:, vcols] for x in held], axis=0)
            for n in range(stacked // step):
                at = slice(g * stacked + n * step, g * stacked + (n + 1) * step)
                h = g * GROUP + 2 * n
                lse = jnp.concatenate([lse_ref[h : h + 1, :], lse_ref[h + 1 : h + 2, :]], axis=1)
                delta = jnp.concatenate([delta_ref[h : h + 1, :], delta_ref[h + 1 : h + 2, :]], axis=1)
                probs = jnp.exp(dot(k, q_ref[at, :], NT) * SCALE - lse)
                p_ref[:height, n * step : (n + 1) * step] = probs.astype(BF16)
                dprob = dot(v, do_ref[at, :], NT)
                ds_ref[row : row + height, at] = (probs * (dprob - delta)).astype(BF16)
            mine = slice(g * stacked, (g + 1) * stacked)
            dk = dot(ds_ref[row : row + height, mine], q_ref[mine, :], NN) * SCALE
            dkv_ref[:height, cols] = dk.astype(BF16)
            dv = dot(p_ref[:height, :], do_ref[mine, :], NN)
            dkv_ref[:height, vcols] = dv.astype(BF16)
        part = dot(dkv_ref[:height, :width], wk_ref[...], NT) + dot(dkv_ref[:height, width:], wv_ref[...], NT)
        at = 0
        for i, x in zip(tile, held):
            size = x.shape[0]
            value = part[at : at + size, :]
            if blocks[i][0][1] == 0:
                near_ref[near_row : near_row + size, :] = value
                near_row += size
            else:
                far_ref[far_row : far_row + size, :] = value.astype(BF16)
                far_row += size
            for b, owner in enumerate(blocks[i]):
                begin = pl.multiple_of(start_ref[index], each)
                src_ref[at + b * each : at + (b + 1) * each, :] = source[owner][pl.ds(begin, each), :]
                index += 1
            at += size
        term = dot(src_ref[:height, :], dkv_ref[:height, width:], TN)
        if fresh:
            total_ref[...] = term
            fresh = False
        elif row == 0:
            total_ref[...] = old_ref[...] + term
        else:
            total_ref[...] += term
        row += height
    if last:
        half = wv_near_ref.shape[0]
        mine = pl.multiple_of(half_ref[0] * half, half)
        other = pl.multiple_of((1 - half_ref[0]) * half, half)
        wv_near_ref[...] = total_ref[pl.ds(mine, half), :]
        wv_far_ref[...] = total_ref[pl.ds(other, half), :].astype(BF16)


def target_kernel(n_chunks, pieces_of, *refs):
    refs = list(refs)
    wq_ref = refs.pop(0)
    ds_refs = refs[:n_chunks]
    n_pieces = sum(pieces_of)
    pieces = refs[n_chunks : n_chunks + n_pieces]
    out_ref, kt_ref = refs[n_chunks + n_pieces :]
    rows = out_ref.shape[0]
    width = kt_ref.shape[0]
    row = 0
    for x in pieces:
        size = x.shape[0]
        kt_ref[:, row : row + size] = x[:, :width].T
        row += size
    total = jnp.zeros((out_ref.shape[1], rows), F32)
    for g in range(KV_HEADS):
        for n in range(GROUP // 2):
            h = g * GROUP + 2 * n
            dq = jnp.zeros((HEAD_DIM, 2 * rows), F32)
            row = 0
            for ds_ref in ds_refs:
                size = ds_ref.shape[0]
                keys = kt_ref[g * HEAD_DIM : (g + 1) * HEAD_DIM, row : row + size]
                dq += dot(keys, ds_ref[:, h * rows : (h + 2) * rows], NN)
                row += size
            dq = (dq * SCALE).astype(BF16)
            for i in range(2):
                cols = slice((h + i) * HEAD_DIM, (h + i + 1) * HEAD_DIM)
                total += dot(wq_ref[:, cols], dq[:, i * rows : (i + 1) * rows], NN)
    out_ref[...] = total.T.astype(BF16)


def place_kernel(n, each, *refs):
    start_ref = refs[0]
    mine, theirs, out_ref = refs[1 : 1 + n], refs[1 + n : 1 + 2 * n], refs[1 + 2 * n]
    index = 0
    for a, b in zip(mine, theirs):
        for at in range(0, a.shape[0], each):
            value = a[at : at + each, :] + b[at : at + each, :].astype(F32)
            out_ref[pl.ds(pl.multiple_of(start_ref[index], each), each), :] = value.astype(BF16)
            index += 1


def gathered(n_sp, n_tp, queries, attn_out, log_norm, cotangent, keys, values, source, w_query, w_key, w_value):
    rows = queries.shape[0]
    each, width = keys.shape
    cols = w_key.shape[0]
    shape = jax.ShapeDtypeStruct
    sp, tp = lax.axis_index("sp"), lax.axis_index("tp")
    core_ring = [(i, i ^ 1) for i in range(n_sp)]
    y_ring = [(i, i ^ 2) for i in range(n_sp)]
    x_ring = [(i, i ^ 1) for i in range(n_tp)]
    up_ring = [(i, (i + 2) % n_tp) for i in range(n_tp)]
    down_ring = [(i, (i - 2) % n_tp) for i in range(n_tp)]

    def core(a):
        return lax.ppermute(a, "sp", core_ring)

    def y(a):
        return lax.ppermute(a, "sp", y_ring)

    def x(a):
        return lax.ppermute(a, "tp", x_ring)

    def up(a):
        return lax.ppermute(a, "tp", up_ring)

    def down(a):
        return lax.ppermute(a, "tp", down_ring)

    own = jnp.concatenate([keys, values], axis=1)
    pair = jnp.concatenate([own, y(own)], axis=0)
    crossed = x(pair)
    below0, above0 = up(pair), down(pair)
    below1, above1 = up(crossed), down(crossed)
    far0, far1 = up(below0), down(above1)

    src_y = y(source)
    src = (source, src_y, core(source), core(src_y))

    qs, dos, delta = call(
        prepare_kernel,
        [shape((HEADS * rows, HEAD_DIM), BF16)] * 2 + [shape((16, rows), F32)],
        [],
        10 * queries.size,
        (queries, cotangent, attn_out),
        name="prepare",
    )
    lse = log_norm.T

    z, lane = tp // 2, tp % 2

    def place(offsets):
        dz, dx = (jnp.asarray(a, jnp.int32) for a in zip(*offsets))
        return (((z + dz) % (n_tp // 2)) * 2 + (lane ^ dx)) * each

    chunks = [
        ([pair, crossed], [(0, 0), (0, 1)]),
        ([below0, below1, above0, above1], [(-1, 0), (-1, 1), (1, 0), (1, 1)]),
        ([far0, far1], [(2, 0), (2, 1)]),
    ]
    half = jnp.reshape(sp % 2, (1,)).astype(jnp.int32)
    total = None
    all_ds, all_pieces, mine, theirs, order = [], [], [], [], []
    for c, (pieces, places) in enumerate(chunks):
        first, last = c == 0, c == len(chunks) - 1
        held, blocks, starts, tiles = [], [], [], []
        for i in range(0, len(pieces), 2):
            tiles.append([len(held) + k for k in range(4)])
            for dc in range(2):
                for k in range(2):
                    held.append(core(pieces[i + k]) if dc else pieces[i + k])
                    blocks.append([(0, dc), (1, dc)])
                    starts += [places[i + k]] * 2
        size = sum(p.shape[0] for p in held)
        height = sum(held[i].shape[0] for i in tiles[0])
        operands = [place(starts), half, lse, delta, qs, dos, w_key, w_value, *src, *held]
        outs = [shape((size, HEADS * rows), BF16), shape((size // 2, cols), F32), shape((size // 2, cols), BF16)]
        scratch = [
            pltpu.VMEM((height, GROUP * rows), BF16),
            pltpu.VMEM((height, 2 * width), BF16),
            pltpu.VMEM((height, cols), BF16),
        ]
        if not first:
            operands.append(total)
        if last:
            outs += [shape((cols // 2, width), F32), shape((cols // 2, width), BF16)]
            scratch.append(pltpu.VMEM((cols, width), F32))
        else:
            outs.append(shape((cols, width), F32))
        flops = 2 * size * rows * HEADS * HEAD_DIM * 4 + 2 * size * cols * width * 3
        results = call(
            functools.partial(chunk_kernel, tiles, blocks, each, first, last),
            outs,
            scratch,
            flops,
            operands,
            specs=[SMEM, SMEM] + [VMEM] * (len(operands) - 2),
            name=f"chunk{c}",
        )
        ds, near, far = results[:3]
        if last:
            wv_near, wv_far = results[3:]
        else:
            total = results[3]
        all_ds.append(ds)
        all_pieces.append(held)
        summed = (near + core(far).astype(F32)).reshape(-1, 2, each, cols)
        mine.append(summed[:, 0].reshape(-1, cols))
        theirs.append(y(summed[:, 1].reshape(-1, cols).astype(BF16)))
        order += places

    wv = (wv_near + core(wv_far).astype(F32)).astype(BF16)
    wv = (wv.astype(F32) + y(wv).astype(F32)).astype(BF16)
    wv_other = core(wv)
    even = sp % 2 == 0
    d_wvalue = jnp.concatenate([jnp.where(even, wv, wv_other), jnp.where(even, wv_other, wv)], axis=0).astype(F32)

    flat = [p for held in all_pieces for p in held]
    (d_target,) = call(
        functools.partial(target_kernel, len(chunks), [len(held) for held in all_pieces]),
        [shape((rows, cols), BF16)],
        [pltpu.VMEM((width, sum(p.shape[0] for p in flat)), BF16)],
        2 * rows * HEADS * HEAD_DIM * (sum(p.shape[0] for p in flat) + cols),
        (w_query, *all_ds, *flat),
        name="target",
    )
    (d_source,) = call(
        functools.partial(place_kernel, len(chunks), each),
        [shape((source.shape[0], cols), BF16)],
        [],
        2 * source.size,
        (place(order), *mine, *theirs),
        specs=[SMEM] + [VMEM] * (2 * len(chunks)),
        name="place",
    )
    return d_target, d_source, d_wvalue


def sharded(queries, attn_out, log_norm, cotangent, keys, values, source, w_query, w_key, w_value):
    rows = queries.shape[0]
    near_keys, near_values = (
        lax.all_gather(keys, "sp", axis=0, tiled=True),
        lax.all_gather(values, "sp", axis=0, tiled=True),
    )
    span = near_keys.shape[0]
    q4 = queries.reshape(rows, KV_HEADS, GROUP, HEAD_DIM)
    g4 = cotangent.reshape(rows, KV_HEADS, GROUP, HEAD_DIM)
    o4 = attn_out.reshape(rows, KV_HEADS, GROUP, HEAD_DIM)
    k3 = near_keys.reshape(span, KV_HEADS, HEAD_DIM)
    v3 = near_values.reshape(span, KV_HEADS, HEAD_DIM)
    delta = jnp.sum(g4.astype(F32) * o4.astype(F32), axis=3)
    delta = jnp.transpose(delta, (1, 2, 0))[..., None]
    lse = jnp.transpose(log_norm.reshape(rows, KV_HEADS, GROUP), (1, 2, 0))[..., None]
    scores = jnp.einsum("znjk,wnk->njzw", q4, k3, preferred_element_type=F32) * SCALE
    probs = jnp.exp(scores - lse)
    probs16 = probs.astype(BF16)
    dprob = jnp.einsum("znjk,wnk->njzw", g4, v3, preferred_element_type=F32)
    dscore = (probs * (dprob - delta)).astype(BF16)
    dq = jnp.einsum("wohn,nwb->hwob", dscore, k3, preferred_element_type=F32) * SCALE
    dk = jnp.einsum("nkjv,jnka->vna", dscore, q4, preferred_element_type=F32) * SCALE
    dv = jnp.einsum("nkjv,jnka->vna", probs16, g4, preferred_element_type=F32)
    own = [
        lax.psum_scatter(a.reshape(span, -1).astype(BF16), "sp", scatter_dimension=0, tiled=True)
        for a in (dk, dv)
    ]
    group = lax.all_gather(jnp.concatenate(own, axis=1), "tp", axis=0, tiled=True)
    weights = jnp.concatenate([w_key, w_value], axis=1)
    d_source = dot(group, weights, NT).astype(BF16)
    term = dot(source, group[:, w_value.shape[1] :], TN)
    d_wvalue = lax.psum(term.astype(BF16), "sp").astype(F32)
    dq16 = lax.psum(dq.reshape(rows, -1), "tp").astype(BF16)
    d_target = dot(dq16, w_query, NT).astype(BF16)
    return d_target, d_source, d_wvalue


def solution(mesh):
    n_sp, n_tp = mesh.shape["sp"], mesh.shape["tp"]

    def shards(*args):
        keys = args[4]
        if (n_sp, n_tp) == (4, 8) and args[0].shape[0] == 128:
            return gathered(n_sp, n_tp, *args)
        return sharded(*args)

    in_specs = (
        P("sp", None),
        P("sp", None),
        P("sp", None),
        P("sp", None),
        P(("sp", "tp"), None),
        P(("sp", "tp"), None),
        P("sp", "tp"),
        P("tp", None),
        P("tp", None),
        P("tp", None),
    )
    out_specs = (P("sp", "tp"), P("sp", "tp"), P("tp", None))
    return jax.shard_map(shards, mesh=mesh, in_specs=in_specs, out_specs=out_specs, check_vma=False)
```

time: 198 us -> 63 us (0.32)
  blocking collectives: 125 us -> 0 us
  starting transfers between devices: 0.12 us -> 23.2 us
  waiting for transfers between devices: 31.6 us -> 17.5 us
  between operations: 13.9 us -> 0.88 us
  Pallas kernels: 0 us -> 12.1 us
  local copies, waits for them, and re-layouts: 15.6 us -> 5.77 us
  matrix products: 8.94 us -> 0 us
    psum x1 -> x0, blocking collectives: 80.8 us -> none  [shards(): dq16 = lax.psum(query_gradient_piece, 'tp').astype(jnp.bfloat16)]
    all_gather x3 -> x0, blocking collectives: 43.8 us -> none  [the longest x1 31.5 us: shards(): group = lax.all_gather(stacked, 'tp', axis=0, tiled=True)]
    psum x1 -> x0, waiting for transfers between devices: 31.5 us -> none  [shards(): lax.psum(weight_term.astype(jnp.bfloat16), 'sp').astype(jnp.float32)]
    ppermute x0 -> x28, starting transfers between devices: none -> 23.2 us  [the longest x6 10.3 us: y(): return lax.ppermute(a, 'sp', y_ring)]
    ppermute x0 -> x28, waiting for transfers between devices: none -> 17.5 us  [the longest x6 7.85 us: y(): return lax.ppermute(a, 'sp', y_ring)]
    pallas_call x0 -> x6, Pallas kernels: none -> 12.1 us  [call(): pl.pallas_call(kernel, out_shape=outs, in_specs=specs or [VMEM] * len(ope...]
    dot_general x8 -> x0, matrix products: 8.94 us -> none  [the longest x1 2.25 us: shards(): lax.dot_general(group, weights, (((1,), (1,)), ((), ())), preferred_eleme...]
    unnamed x24 -> x20, local copies, waits for them, and re-layouts: 10.6 us -> 4.95 us
  transfers between devices with their start and end apart: 3 -> 28, of which waited for: 1 -> 7; matrix products, arithmetic and copies ran while one was open for 7% -> 4% of each run, Pallas kernels for 0% -> 19%
where the time goes in v1:
time: 63 us; the launch traced here: 62.6 us
  starting transfers between devices  23.2 us (37%)
  waiting for transfers between devices  17.5 us (28%)
  Pallas kernels  12.1 us (19%)
  local copies, waits for them, and re-layouts  5.77 us (9%)
  other arithmetic  3.21 us (5%)
  between operations  0.88 us (1%)
    pallas_call x6, Pallas kernels, call(): pl.pallas_call(kernel, out_shape=outs, in_specs=specs or [VMEM] * len(ope...  12.1 us
    ppermute x6, starting transfers between devices, y(): return lax.ppermute(a, 'sp', y_ring)  10.3 us
    ppermute x3, starting transfers between devices, down(): return lax.ppermute(a, 'tp', down_ring)  8.44 us
    ppermute x6, waiting for transfers between devices, y(): return lax.ppermute(a, 'sp', y_ring)  7.85 us
    unnamed x20, local copies, waits for them, and re-layouts  4.95 us
    ppermute x3, waiting for transfers between devices, up(): return lax.ppermute(a, 'tp', up_ring)  4.38 us
    ppermute x15, starting transfers between devices, core(): return lax.ppermute(a, 'sp', core_ring)  2.95 us
    ppermute x1, waiting for transfers between devices, x(): return lax.ppermute(a, 'tp', x_ring)  2.79 us
  transfers between devices with their start and end apart: 28, of which 7 were waited for; matrix products, arithmetic and copies ran while one was open for 4% of the time, Pallas kernels for 19%

profile of v1, /device:TPU:0, one launch (start us, length us, event | category | flops | bytes accessed | tf_op | source)
XLA Modules:
  0.0 62.6 jit_solution(14712830160175899381)
XLA Ops:
  0.7 0.8 %constant_dynamic-update-slice_fusion.1 = bf16[32,1024]{1,0:T(8,128)(2,1)S(1)} fusion(bf16[32,512]{1,0:T(8,128)(2,1)} %param.22), kind=kLoop, calls=%fused_computation.13 | loop fusion | bytes 65536
  1.5 0.8 %constant_dynamic-update-slice_fusion = bf16[32,1024]{1,0:T(8,128)(2,1)S(1)} fusion(bf16[32,1024]{1,0:T(8,128)(2,1)S(1)} %constant_dynamic-update-slice_fusion.1, bf16[32,512]{1,0:T(8,128)(2,1)} %param.23), kind=kLoop, calls=%fused_computation.12 | loop fusion | bytes 65536 | tf_op jit(solution)/shard_map/concatenate | solution.py:212
  2.2 3.0 %collective-permute-start.3 = (bf16[32,1024]{1,0:T(8,128)(2,1)S(1)}, bf16[32,1024]{1,0:T(8,128)(2,1)S(1)}, u32[]{:S(2)}, u32[]{:S(2)}) collective-permute-start(bf16[32,1024]{1,0:T(8,128)(2,1)S(1)} %constant_dynamic-update-slice_fusion), channel_id=1, source_target_pairs={{0,16},{8,24},{16,0},{24,8},{1,17},{9,25},{17,1},{25,9},{2,18},{10... | collective-permute-start | bytes 196616 | tf_op jit(solution)/shard_map/ppermute | solution.py:201
  5.2 2.2 %collective-permute-done.3 = bf16[32,1024]{1,0:T(8,128)(2,1)S(1)} collective-permute-done((bf16[32,1024]{1,0:T(8,128)(2,1)S(1)}, bf16[32,1024]{1,0:T(8,128)(2,1)S(1)}, u32[]{:S(2)}, u32[]{:S(2)}) %collective-permute-start.3) | collective-permute-done | bytes 65568 | tf_op jit(solution)/shard_map/ppermute | solution.py:201
  7.5 4.2 %collective-permute-start.11 = (bf16[64,1024]{1,0:T(8,128)(2,1)S(1)}, bf16[64,1024]{1,0:T(8,128)(2,1)S(1)}, u32[]{:S(2)}, u32[]{:S(2)}) collective-permute-start(bf16[64,1024]{1,0:T(8,128)(2,1)S(1)} %pad_maximum_fusion.refs_12_.refs_4_), channel_id=1, source_target_pairs={{0,6},{1,7},{2,0},{3,1},{4,2},{5,3},{6,4},{7,5},{8,14},{9,15},{10,... | collective-permute-start | bytes 393224 | tf_op jit(solution)/shard_map/ppermute | solution.py:210
  11.6 1.5 %collective-permute-start = (bf16[256,384]{1,0:T(8,128)(2,1)}, bf16[256,384]{1,0:T(8,128)(2,1)S(1)}, u32[]{:S(2)}, u32[]{:S(2)}) collective-permute-start(bf16[256,384]{1,0:T(8,128)(2,1)} %refs_8_.5), channel_id=1, source_target_pairs={{0,16},{8,24},{16,0},{24,8},{1,17},{9,25},{17,1},{25,9},{2,18},{10... | collective-permute-start | bytes 589832 | tf_op jit(solution)/shard_map/ppermute | solution.py:201
  13.4 1.2 %collective-permute-done.11.refs_16_.refs_12_ = bf16[64,1024]{1,0:T(8,128)(2,1)S(1)} collective-permute-done((bf16[64,1024]{1,0:T(8,128)(2,1)S(1)}, bf16[64,1024]{1,0:T(8,128)(2,1)S(1)}, u32[]{:S(2)}, u32[]{:S(2)}) %collective-permute-start.11) | collective-permute-done | bytes 131104 | tf_op jit(solution)/shard_map/ppermute | solution.py:210
  14.5 1.5 %collective-permute-start.4 = (bf16[64,1024]{1,0:T(8,128)(2,1)S(1)}, bf16[64,1024]{1,0:T(8,128)(2,1)S(1)}, u32[]{:S(2)}, u32[]{:S(2)}) collective-permute-start(bf16[64,1024]{1,0:T(8,128)(2,1)S(1)} %pad_maximum_fusion.refs_12_.refs_4_), channel_id=1, source_target_pairs={{0,1},{1,0},{2,3},{3,2},{4,5},{5,4},{6,7},{7,6},{8,9},{9,8},{10,11... | collective-permute-start | bytes 393224 | tf_op jit(solution)/shard_map/ppermute | solution.py:204
  16.0 0.7 %fusion.9.refs_0_ = s32[16]{0:T(128)S(1)} fusion(s32[16]{0:T(128)} %constant.92.clone, s32[16]{0:T(128)} %constant.93.clone, s32[]{:T(128)S(6)} %select_n.51, s32[]{:T(128)S(6)} %select_n.49), kind=kLoop, calls=%fused_computation.31 | loop fusion | flops 256 | bytes 200 | tf_op jit(solution)/shard_map/mul | solution.py:236
  16.7 2.8 %collective-permute-done.4.refs_13_.refs_5_ = bf16[64,1024]{1,0:T(8,128)(2,1)S(1)} collective-permute-done((bf16[64,1024]{1,0:T(8,128)(2,1)S(1)}, bf16[64,1024]{1,0:T(8,128)(2,1)S(1)}, u32[]{:S(2)}, u32[]{:S(2)}) %collective-permute-start.4) | collective-permute-done | bytes 131104 | tf_op jit(solution)/shard_map/ppermute | solution.py:204
  19.5 4.3 %collective-permute-start.12 = (bf16[64,1024]{1,0:T(8,128)(2,1)S(1)}, bf16[64,1024]{1,0:T(8,128)(2,1)S(1)}, u32[]{:S(2)}, u32[]{:S(2)}) collective-permute-start(bf16[64,1024]{1,0:T(8,128)(2,1)S(1)} %collective-permute-done.4.refs_13_.refs_5_), channel_id=1, source_target_pairs={{0,6},{1,7},{2,0},{3,1},{4,2},{5,3},{6,4},{7,5},{8,14},{9,15},{10,... | collective-permute-start | bytes 393224 | tf_op jit(solution)/shard_map/ppermute | solution.py:210
  23.9 0.5 collective-permute-start.13
  24.5 0.7 %fusion.8.refs_0_ = s32[8]{0:T(128)S(1)} fusion(s32[8]{0:T(128)} %constant.95.clone, s32[8]{0:T(128)} %constant.96.clone, s32[]{:T(128)S(6)} %select_n.51, s32[]{:T(128)S(6)} %select_n.49), kind=kLoop, calls=%fused_computation.30 | loop fusion | flops 128 | bytes 104 | tf_op jit(solution)/shard_map/mul | solution.py:236
  25.4 1.0 %collective-permute-done.12.refs_17_.refs_13_ = bf16[64,1024]{1,0:T(8,128)(2,1)S(1)} collective-permute-done((bf16[64,1024]{1,0:T(8,128)(2,1)S(1)}, bf16[64,1024]{1,0:T(8,128)(2,1)S(1)}, u32[]{:S(2)}, u32[]{:S(2)}) %collective-permute-start.12) | collective-permute-done | bytes 131104 | tf_op jit(solution)/shard_map/ppermute | solution.py:210
  26.4 4.4 %collective-permute-done.8.refs_13_.refs_9_ = bf16[64,1024]{1,0:T(8,128)(2,1)S(1)} collective-permute-done((bf16[64,1024]{1,0:T(8,128)(2,1)S(1)}, bf16[64,1024]{1,0:T(8,128)(2,1)S(1)}, u32[]{:S(2)}, u32[]{:S(2)}) %collective-permute-start.8) | collective-permute-done | bytes 131104 | tf_op jit(solution)/shard_map/ppermute | solution.py:207
  31.3 0.7 %fusion.1 = (s32[8]{0:T(128)S(1)}, s32[8]{0:T(128)S(1)}) fusion(s32[8]{0:T(128)} %constant.91.clone, s32[]{:T(128)S(6)} %mul.33, s32[]{:T(128)S(6)} %select_n.51, s32[]{:T(128)S(6)} %mul.32), kind=kLoop, calls=%fused_computation.23 | loop fusion | flops 40 | bytes 108 | tf_op jit(solution)/shard_map/mul | solution.py:236
  32.0 1.1 %copy-done.1 = bf16[128,3072]{1,0:T(8,128)(2,1)S(1)} copy-done((bf16[128,3072]{1,0:T(8,128)(2,1)S(1)}, bf16[128,3072]{1,0:T(8,128)(2,1)}, u32[]{:S(2)}) %copy-start.1) | copy-done | bytes 786456
  33.1 1.1 %copy-done.2 = bf16[128,3072]{1,0:T(8,128)(2,1)S(1)} copy-done((bf16[128,3072]{1,0:T(8,128)(2,1)S(1)}, bf16[128,3072]{1,0:T(8,128)(2,1)}, u32[]{:S(2)}) %copy-start.2) | copy-done | bytes 786456
  34.3 1.1 %copy-done.3 = bf16[128,3072]{1,0:T(8,128)(2,1)S(1)} copy-done((bf16[128,3072]{1,0:T(8,128)(2,1)S(1)}, bf16[128,3072]{1,0:T(8,128)(2,1)}, u32[]{:S(2)}) %copy-start.3) | copy-done | bytes 786456
  35.7 0.7 %copy-done.5 = bf16[384,512]{1,0:T(8,128)(2,1)S(1)} copy-done((bf16[384,512]{1,0:T(8,128)(2,1)S(1)}, bf16[384,512]{1,0:T(8,128)(2,1)}, u32[]{:S(2)}) %copy-start.5) | copy-done | bytes 393240
  36.4 2.0 %chunk0.1 = (bf16[256,1536]{1,0:T(8,128)(2,1)S(1)}, f32[128,384]{1,0:T(8,128)S(1)}, bf16[128,384]{1,0:T(8,128)(2,1)S(1)}, f32[384,512]{1,0:T(8,128)S(1)}) custom-call(s32[8]{0:T(128)S(1)} %get-tuple-element.38.refs_0_, s32[1]{0:T(128)} %bitcast.refs_1_, f32[12,128]{1,0:T(8,128)S(1)} %bitcast.20, f32[16,128]{1,0:T(8,128)S(1)} %get-tuple-element.19.refs_3_, ...), custom_call_target="tpu_custom_call" | custom-call | flops 1107296256 | bytes 5552164 | tf_op jit(solution)/shard_map/chunk0/pallas_call | solution.py:34
  39.2 3.2 %chunk1.1 = (bf16[512,1536]{1,0:T(8,128)(2,1)S(1)}, f32[256,384]{1,0:T(8,128)S(1)}, bf16[256,384]{1,0:T(8,128)(2,1)S(1)}, f32[384,512]{1,0:T(8,128)S(1)}) custom-call(s32[16]{0:T(128)S(1)} %fusion.9.refs_0_, s32[1]{0:T(128)} %bitcast.refs_1_, f32[12,128]{1,0:T(8,128)S(1)} %bitcast.21, f32[16,128]{1,0:T(8,128)S(1)} %get-tuple-element.19.refs_3_, ...), custom_call_target="tpu_custom_call" | custom-call | flops 2214592512 | bytes 7944260 | tf_op jit(solution)/shard_map/chunk1/pallas_call | solution.py:34
  42.4 0.4 collective-permute-start.20
  42.8 2.0 %chunk2.1 = (bf16[256,1536]{1,0:T(8,128)(2,1)S(1)}, f32[128,384]{1,0:T(8,128)S(1)}, bf16[128,384]{1,0:T(8,128)(2,1)S(1)}, f32[192,512]{1,0:T(8,128)S(1)}, bf16[192,512]{1,0:T(8,128)(2,1)S(1)}) custom-call(s32[8]{0:T(128)S(1)} %get-tuple-element.37.refs_0_, s32[1]{0:T(128)} %bitcast.refs_1_, f32[12,128]{1,0:T(8,128)S(1)} %bitcast.22, ...), custom_call_target="tpu_custom_call" | custom-call | flops 1107296256 | bytes 6141988 | tf_op jit(solution)/shard_map/chunk2/pallas_call | solution.py:34
  45.1 2.5 %collective-permute-start.22 = (bf16[64,384]{1,0:T(8,128)(2,1)S(1)}, bf16[64,384]{1,0:T(8,128)(2,1)S(1)}, u32[]{:S(2)}, u32[]{:S(2)}) collective-permute-start(bf16[64,384]{1,0:T(8,128)(2,1)S(1)} %bitcast.30), channel_id=1, source_target_pairs={{0,16},{8,24},{16,0},{24,8},{1,17},{9,25},{17,1},{25,9},{2,18},{10... | collective-permute-start | bytes 147464 | tf_op jit(solution)/shard_map/ppermute | solution.py:201
  47.9 1.1 %collective-permute-start.26 = (bf16[192,512]{1,0:T(8,128)(2,1)S(1)}, bf16[192,512]{1,0:T(8,128)(2,1)S(1)}, u32[]{:S(2)}, u32[]{:S(2)}) collective-permute-start(bf16[192,512]{1,0:T(8,128)(2,1)S(1)} %add_convert_fusion.1), channel_id=1, source_target_pairs={{0,16},{8,24},{16,0},{24,8},{1,17},{9,25},{17,1},{25,9},{2,18},{10... | collective-permute-start | bytes 589832 | tf_op jit(solution)/shard_map/ppermute | solution.py:201
  49.1 1.0 %collective-permute-start.23 = (bf16[128,384]{1,0:T(8,128)(2,1)S(1)}, bf16[128,384]{1,0:T(8,128)(2,1)S(1)}, u32[]{:S(2)}, u32[]{:S(2)}) collective-permute-start(bf16[128,384]{1,0:T(8,128)(2,1)S(1)} %bitcast.29), channel_id=1, source_target_pairs={{0,16},{8,24},{16,0},{24,8},{1,17},{9,25},{17,1},{25,9},{2,18},{10... | collective-permute-start | bytes 294920 | tf_op jit(solution)/shard_map/ppermute | solution.py:201
  50.1 5.6 %collective-permute-done.26 = bf16[192,512]{1,0:T(8,128)(2,1)S(1)} collective-permute-done((bf16[192,512]{1,0:T(8,128)(2,1)S(1)}, bf16[192,512]{1,0:T(8,128)(2,1)S(1)}, u32[]{:S(2)}, u32[]{:S(2)}) %collective-permute-start.26) | collective-permute-done | bytes 196640 | tf_op jit(solution)/shard_map/ppermute | solution.py:201
  55.9 1.1 %collective-permute-start.24 = (bf16[64,384]{1,0:T(8,128)(2,1)S(1)}, bf16[64,384]{1,0:T(8,128)(2,1)S(1)}, u32[]{:S(2)}, u32[]{:S(2)}) collective-permute-start(bf16[64,384]{1,0:T(8,128)(2,1)S(1)} %bitcast.31), channel_id=1, source_target_pairs={{0,16},{8,24},{16,0},{24,8},{1,17},{9,25},{17,1},{25,9},{2,18},{10... | collective-permute-start | bytes 147464 | tf_op jit(solution)/shard_map/ppermute | solution.py:201
  57.0 3.3 %target.1 = bf16[128,384]{1,0:T(8,128)(2,1)} custom-call(bf16[384,3072]{1,0:T(8,128)(2,1)S(1)} %copy-done, bf16[256,1536]{1,0:T(8,128)(2,1)S(1)} %get-tuple-element.22.refs_1_, bf16[512,1536]{1,0:T(8,128)(2,1)S(1)} %get-tuple-element.24.refs_2_, bf16[256,1536]{1,0:T(8,128)(2,1)S(1)} %get-tuple-element.26.refs_3_, ...), custom_call_target="tpu_custom_call" | custom-call | flops 1107296256 | bytes 7700480 | tf_op jit(solution)/shard_map/target/pallas_call | solution.py:34
  60.4 1.3 %place.1 = bf16[256,384]{1,0:T(8,128)(2,1)} custom-call(s32[8]{0:T(128)S(1)} %fusion.8.refs_0_, f32[64,384]{1,0:T(8,128)S(1)} %bitcast.18, f32[128,384]{1,0:T(8,128)S(1)} %bitcast.17, f32[64,384]{1,0:T(8,128)S(1)} %bitcast.19, bf16[64,384]{1,0:T(8,128)(2,1)S(1)} %collective-permute-done.22.refs_4_, bf16[128,384]{1,0:T(8,128)(2,1)S(1)} %collective-permute-done.23.refs_5_, ...), custom_call_target="tpu_custom_call" | custom-call | flops 196608 | bytes 786464 | tf_op jit(solution)/shard_map/place/pallas_call | solution.py:34
  61.7 1.0 %maximum_convert_fusion = f32[384,512]{1,0:T(8,128)} fusion(bf16[192,512]{1,0:T(8,128)(2,1)S(1)} %get-tuple-element.36, bf16[192,512]{1,0:T(8,128)(2,1)S(1)} %get-tuple-element.35), kind=kLoop, calls=%fused_computation | loop fusion | flops 786432 | bytes 1179648 | tf_op jit(solution)/shard_map/convert_element_type | solution.py:298
  (68 shorter events, 3.0 us)
Async XLA Ops:
  0.6 35.1 %copy-start.4 = (bf16[384,512]{1,0:T(8,128)(2,1)S(1)}, bf16[384,512]{1,0:T(8,128)(2,1)}, u32[]{:S(2)}) copy-start(bf16[384,512]{1,0:T(8,128)(2,1)} %refs_6_.5) | copy-start | bytes 1179652
  0.6 35.1 %copy-start.7 = (f32[128,12]{0,1:T(8,128)S(1)}, f32[128,12]{0,1:T(8,128)}, u32[]{:S(2)}) copy-start(f32[128,12]{0,1:T(8,128)} %param.20) | copy-start | bytes 18436
  2.2 5.2 %collective-permute-start.3 = (bf16[32,1024]{1,0:T(8,128)(2,1)S(1)}, bf16[32,1024]{1,0:T(8,128)(2,1)S(1)}, u32[]{:S(2)}, u32[]{:S(2)}) collective-permute-start(bf16[32,1024]{1,0:T(8,128)(2,1)S(1)} %constant_dynamic-update-slice_fusion), channel_id=1, source_target_pairs={{0,16},{8,24},{16,0},{24,8},{1,17},{9,25},{17,1},{25,9},{2,18},{10... | collective-permute-start | bytes 196616 | tf_op jit(solution)/shard_map/ppermute | solution.py:201
  7.5 7.1 %collective-permute-start.11 = (bf16[64,1024]{1,0:T(8,128)(2,1)S(1)}, bf16[64,1024]{1,0:T(8,128)(2,1)S(1)}, u32[]{:S(2)}, u32[]{:S(2)}) collective-permute-start(bf16[64,1024]{1,0:T(8,128)(2,1)S(1)} %pad_maximum_fusion.refs_12_.refs_4_), channel_id=1, source_target_pairs={{0,6},{1,7},{2,0},{3,1},{4,2},{5,3},{6,4},{7,5},{8,14},{9,15},{10,... | collective-permute-start | bytes 393224 | tf_op jit(solution)/shard_map/ppermute | solution.py:210
  11.6 12.3 %collective-permute-start.1 = (bf16[256,384]{1,0:T(8,128)(2,1)}, bf16[256,384]{1,0:T(8,128)(2,1)S(1)}, u32[]{:S(2)}, u32[]{:S(2)}) collective-permute-start(bf16[256,384]{1,0:T(8,128)(2,1)} %refs_8_.5), channel_id=1, source_target_pairs={{0,8},{8,0},{16,24},{24,16},{1,9},{9,1},{17,25},{25,17},{2,10},{10... | collective-permute-start | bytes 589832 | tf_op jit(solution)/shard_map/ppermute | solution.py:198
  11.6 12.8 %collective-permute-start = (bf16[256,384]{1,0:T(8,128)(2,1)}, bf16[256,384]{1,0:T(8,128)(2,1)S(1)}, u32[]{:S(2)}, u32[]{:S(2)}) collective-permute-start(bf16[256,384]{1,0:T(8,128)(2,1)} %refs_8_.5), channel_id=1, source_target_pairs={{0,16},{8,24},{16,0},{24,8},{1,17},{9,25},{17,1},{25,9},{2,18},{10... | collective-permute-start | bytes 589832 | tf_op jit(solution)/shard_map/ppermute | solution.py:201
  13.2 10.7 %collective-permute-start.7 = (bf16[64,1024]{1,0:T(8,128)(2,1)S(1)}, bf16[64,1024]{1,0:T(8,128)(2,1)S(1)}, u32[]{:S(2)}, u32[]{:S(2)}) collective-permute-start(bf16[64,1024]{1,0:T(8,128)(2,1)S(1)} %pad_maximum_fusion.refs_12_.refs_4_), channel_id=1, source_target_pairs={{0,2},{1,3},{2,4},{3,5},{4,6},{5,7},{6,0},{7,1},{8,10},{9,11},{10,... | collective-permute-start | bytes 393224 | tf_op jit(solution)/shard_map/ppermute | solution.py:207
  13.2 10.7 %collective-permute-start.5 = (bf16[64,1024]{1,0:T(8,128)(2,1)S(1)}, bf16[64,1024]{1,0:T(8,128)(2,1)S(1)}, u32[]{:S(2)}, u32[]{:S(2)}) collective-permute-start(bf16[64,1024]{1,0:T(8,128)(2,1)S(1)} %pad_maximum_fusion.refs_12_.refs_4_), channel_id=1, source_target_pairs={{0,8},{8,0},{16,24},{24,16},{1,9},{9,1},{17,25},{25,17},{2,10},{10... | collective-permute-start | bytes 393224 | tf_op jit(solution)/shard_map/ppermute | solution.py:198
  14.5 5.0 %collective-permute-start.4 = (bf16[64,1024]{1,0:T(8,128)(2,1)S(1)}, bf16[64,1024]{1,0:T(8,128)(2,1)S(1)}, u32[]{:S(2)}, u32[]{:S(2)}) collective-permute-start(bf16[64,1024]{1,0:T(8,128)(2,1)S(1)} %pad_maximum_fusion.refs_12_.refs_4_), channel_id=1, source_target_pairs={{0,1},{1,0},{2,3},{3,2},{4,5},{5,4},{6,7},{7,6},{8,9},{9,8},{10,11... | collective-permute-start | bytes 393224 | tf_op jit(solution)/shard_map/ppermute | solution.py:204
  19.5 6.9 %collective-permute-start.12 = (bf16[64,1024]{1,0:T(8,128)(2,1)S(1)}, bf16[64,1024]{1,0:T(8,128)(2,1)S(1)}, u32[]{:S(2)}, u32[]{:S(2)}) collective-permute-start(bf16[64,1024]{1,0:T(8,128)(2,1)S(1)} %collective-permute-done.4.refs_13_.refs_5_), channel_id=1, source_target_pairs={{0,6},{1,7},{2,0},{3,1},{4,2},{5,3},{6,4},{7,5},{8,14},{9,15},{10,... | collective-permute-start | bytes 393224 | tf_op jit(solution)/shard_map/ppermute | solution.py:210
  23.8 7.0 %collective-permute-start.8 = (bf16[64,1024]{1,0:T(8,128)(2,1)S(1)}, bf16[64,1024]{1,0:T(8,128)(2,1)S(1)}, u32[]{:S(2)}, u32[]{:S(2)}) collective-permute-start(bf16[64,1024]{1,0:T(8,128)(2,1)S(1)} %collective-permute-done.4.refs_13_.refs_5_), channel_id=1, source_target_pairs={{0,2},{1,3},{2,4},{3,5},{4,6},{5,7},{6,0},{7,1},{8,10},{9,11},{10,... | collective-permute-start | bytes 393224 | tf_op jit(solution)/shard_map/ppermute | solution.py:207
  23.8 7.0 %collective-permute-start.6 = (bf16[64,1024]{1,0:T(8,128)(2,1)S(1)}, bf16[64,1024]{1,0:T(8,128)(2,1)S(1)}, u32[]{:S(2)}, u32[]{:S(2)}) collective-permute-start(bf16[64,1024]{1,0:T(8,128)(2,1)S(1)} %collective-permute-done.4.refs_13_.refs_5_), channel_id=1, source_target_pairs={{0,8},{8,0},{16,24},{24,16},{1,9},{9,1},{17,25},{25,17},{2,10},{10... | collective-permute-start | bytes 393224 | tf_op jit(solution)/shard_map/ppermute | solution.py:198
  23.9 1.5 %collective-permute-start.13 = (bf16[64,1024]{1,0:T(8,128)(2,1)S(1)}, bf16[64,1024]{1,0:T(8,128)(2,1)S(1)}, u32[]{:S(2)}, u32[]{:S(2)}) collective-permute-start(bf16[64,1024]{1,0:T(8,128)(2,1)S(1)} %collective-permute-done.11.refs_16_.refs_12_), channel_id=1, source_target_pairs={{0,8},{8,0},{16,24},{24,16},{1,9},{9,1},{17,25},{25,17},{2,10},{10... | collective-permute-start | bytes 393224 | tf_op jit(solution)/shard_map/ppermute | solution.py:198
  24.4 6.6 %collective-permute-start.2 = (bf16[256,384]{1,0:T(8,128)(2,1)S(1)}, bf16[256,384]{1,0:T(8,128)(2,1)S(1)}, u32[]{:S(2)}, u32[]{:S(2)}) collective-permute-start(bf16[256,384]{1,0:T(8,128)(2,1)S(1)} %collective-permute-done.refs_9_), channel_id=1, source_target_pairs={{0,8},{8,0},{16,24},{24,16},{1,9},{9,1},{17,25},{25,17},{2,10},{10... | collective-permute-start | bytes 589832 | tf_op jit(solution)/shard_map/ppermute | solution.py:198
  25.4 13.0 %collective-permute-start.15 = (bf16[64,1024]{1,0:T(8,128)(2,1)S(1)}, bf16[64,1024]{1,0:T(8,128)(2,1)S(1)}, u32[]{:S(2)}, u32[]{:S(2)}) collective-permute-start(bf16[64,1024]{1,0:T(8,128)(2,1)S(1)} %collective-permute-done.7.refs_12_.refs_8_), channel_id=1, source_target_pairs={{0,2},{1,3},{2,4},{3,5},{4,6},{5,7},{6,0},{7,1},{8,10},{9,11},{10,... | collective-permute-start | bytes 393224 | tf_op jit(solution)/shard_map/ppermute | solution.py:207
  26.4 12.2 %collective-permute-start.9 = (bf16[64,1024]{1,0:T(8,128)(2,1)S(1)}, bf16[64,1024]{1,0:T(8,128)(2,1)S(1)}, u32[]{:S(2)}, u32[]{:S(2)}) collective-permute-start(bf16[64,1024]{1,0:T(8,128)(2,1)S(1)} %collective-permute-done.7.refs_12_.refs_8_), channel_id=1, source_target_pairs={{0,8},{8,0},{16,24},{24,16},{1,9},{9,1},{17,25},{25,17},{2,10},{10... | collective-permute-start | bytes 393224 | tf_op jit(solution)/shard_map/ppermute | solution.py:198
  30.8 8.2 %collective-permute-start.16 = (bf16[64,1024]{1,0:T(8,128)(2,1)S(1)}, bf16[64,1024]{1,0:T(8,128)(2,1)S(1)}, u32[]{:S(2)}, u32[]{:S(2)}) collective-permute-start(bf16[64,1024]{1,0:T(8,128)(2,1)S(1)} %collective-permute-done.12.refs_17_.refs_13_), channel_id=1, source_target_pairs={{0,6},{1,7},{2,0},{3,1},{4,2},{5,3},{6,4},{7,5},{8,14},{9,15},{10,... | collective-permute-start | bytes 393224 | tf_op jit(solution)/shard_map/ppermute | solution.py:210
  30.8 8.3 %collective-permute-start.14 = (bf16[64,1024]{1,0:T(8,128)(2,1)S(1)}, bf16[64,1024]{1,0:T(8,128)(2,1)S(1)}, u32[]{:S(2)}, u32[]{:S(2)}) collective-permute-start(bf16[64,1024]{1,0:T(8,128)(2,1)S(1)} %collective-permute-done.12.refs_17_.refs_13_), channel_id=1, source_target_pairs={{0,8},{8,0},{16,24},{24,16},{1,9},{9,1},{17,25},{25,17},{2,10},{10... | collective-permute-start | bytes 393224 | tf_op jit(solution)/shard_map/ppermute | solution.py:198
  31.0 8.2 %collective-permute-start.10 = (bf16[64,1024]{1,0:T(8,128)(2,1)S(1)}, bf16[64,1024]{1,0:T(8,128)(2,1)S(1)}, u32[]{:S(2)}, u32[]{:S(2)}) collective-permute-start(bf16[64,1024]{1,0:T(8,128)(2,1)S(1)} %collective-permute-done.8.refs_13_.refs_9_), channel_id=1, source_target_pairs={{0,8},{8,0},{16,24},{24,16},{1,9},{9,1},{17,25},{25,17},{2,10},{10... | collective-permute-start | bytes 393224 | tf_op jit(solution)/shard_map/ppermute | solution.py:198
  32.0 1.1 %copy-start.1 = (bf16[128,3072]{1,0:T(8,128)(2,1)S(1)}, bf16[128,3072]{1,0:T(8,128)(2,1)}, u32[]{:S(2)}) copy-start(bf16[128,3072]{1,0:T(8,128)(2,1)} %q_ref.1) | copy-start | bytes 2359300
  38.4 4.4 %collective-permute-start.17 = (bf16[64,1024]{1,0:T(8,128)(2,1)S(1)}, bf16[64,1024]{1,0:T(8,128)(2,1)S(1)}, u32[]{:S(2)}, u32[]{:S(2)}) collective-permute-start(bf16[64,1024]{1,0:T(8,128)(2,1)S(1)} %collective-permute-done.15.refs_12_.refs_16_), channel_id=1, source_target_pairs={{0,8},{8,0},{16,24},{24,16},{1,9},{9,1},{17,25},{25,17},{2,10},{10... | collective-permute-start | bytes 393224 | tf_op jit(solution)/shard_map/ppermute | solution.py:198
  38.6 6.4 %collective-permute-start.19 = (bf16[128,384]{1,0:T(8,128)(2,1)S(1)}, bf16[128,384]{1,0:T(8,128)(2,1)S(1)}, u32[]{:S(2)}, u32[]{:S(2)}) collective-permute-start(bf16[128,384]{1,0:T(8,128)(2,1)S(1)} %get-tuple-element.28), channel_id=1, source_target_pairs={{0,8},{8,0},{16,24},{24,16},{1,9},{9,1},{17,25},{25,17},{2,10},{10... | collective-permute-start | bytes 294920 | tf_op jit(solution)/shard_map/ppermute | solution.py:198
  39.0 3.8 %collective-permute-start.18 = (bf16[64,1024]{1,0:T(8,128)(2,1)S(1)}, bf16[64,1024]{1,0:T(8,128)(2,1)S(1)}, u32[]{:S(2)}, u32[]{:S(2)}) collective-permute-start(bf16[64,1024]{1,0:T(8,128)(2,1)S(1)} %collective-permute-done.16.refs_13_.refs_17_), channel_id=1, source_target_pairs={{0,8},{8,0},{16,24},{24,16},{1,9},{9,1},{17,25},{25,17},{2,10},{10... | collective-permute-start | bytes 393224 | tf_op jit(solution)/shard_map/ppermute | solution.py:198
  42.4 6.6 %collective-permute-start.20 = (bf16[256,384]{1,0:T(8,128)(2,1)S(1)}, bf16[256,384]{1,0:T(8,128)(2,1)S(1)}, u32[]{:S(2)}, u32[]{:S(2)}) collective-permute-start(bf16[256,384]{1,0:T(8,128)(2,1)S(1)} %get-tuple-element.30), channel_id=1, source_target_pairs={{0,8},{8,0},{16,24},{24,16},{1,9},{9,1},{17,25},{25,17},{2,10},{10... | collective-permute-start | bytes 589832 | tf_op jit(solution)/shard_map/ppermute | solution.py:198
  44.9 12.2 %copy-start = (bf16[384,3072]{1,0:T(8,128)(2,1)S(1)}, bf16[384,3072]{1,0:T(8,128)(2,1)}, u32[]{:S(2)}) copy-start(bf16[384,3072]{1,0:T(8,128)(2,1)} %refs_0_.1) | copy-start | bytes 7077892
  44.9 2.9 %collective-permute-start.25 = (bf16[192,512]{1,0:T(8,128)(2,1)S(1)}, bf16[192,512]{1,0:T(8,128)(2,1)S(1)}, u32[]{:S(2)}, u32[]{:S(2)}) collective-permute-start(bf16[192,512]{1,0:T(8,128)(2,1)S(1)} %get-tuple-element.34), channel_id=1, source_target_pairs={{0,8},{8,0},{16,24},{24,16},{1,9},{9,1},{17,25},{25,17},{2,10},{10... | collective-permute-start | bytes 589832 | tf_op jit(solution)/shard_map/ppermute | solution.py:198
  45.1 15.2 %collective-permute-start.22 = (bf16[64,384]{1,0:T(8,128)(2,1)S(1)}, bf16[64,384]{1,0:T(8,128)(2,1)S(1)}, u32[]{:S(2)}, u32[]{:S(2)}) collective-permute-start(bf16[64,384]{1,0:T(8,128)(2,1)S(1)} %bitcast.30), channel_id=1, source_target_pairs={{0,16},{8,24},{16,0},{24,8},{1,17},{9,25},{17,1},{25,9},{2,18},{10... | collective-permute-start | bytes 147464 | tf_op jit(solution)/shard_map/ppermute | solution.py:201
  47.7 8.2 %collective-permute-start.21 = (bf16[128,384]{1,0:T(8,128)(2,1)S(1)}, bf16[128,384]{1,0:T(8,128)(2,1)S(1)}, u32[]{:S(2)}, u32[]{:S(2)}) collective-permute-start(bf16[128,384]{1,0:T(8,128)(2,1)S(1)} %get-tuple-element.32), channel_id=1, source_target_pairs={{0,8},{8,0},{16,24},{24,16},{1,9},{9,1},{17,25},{25,17},{2,10},{10... | collective-permute-start | bytes 294920 | tf_op jit(solution)/shard_map/ppermute | solution.py:198
  47.9 7.8 %collective-permute-start.26 = (bf16[192,512]{1,0:T(8,128)(2,1)S(1)}, bf16[192,512]{1,0:T(8,128)(2,1)S(1)}, u32[]{:S(2)}, u32[]{:S(2)}) collective-permute-start(bf16[192,512]{1,0:T(8,128)(2,1)S(1)} %add_convert_fusion.1), channel_id=1, source_target_pairs={{0,16},{8,24},{16,0},{24,8},{1,17},{9,25},{17,1},{25,9},{2,18},{10... | collective-permute-start | bytes 589832 | tf_op jit(solution)/shard_map/ppermute | solution.py:201
  49.1 11.3 %collective-permute-start.23 = (bf16[128,384]{1,0:T(8,128)(2,1)S(1)}, bf16[128,384]{1,0:T(8,128)(2,1)S(1)}, u32[]{:S(2)}, u32[]{:S(2)}) collective-permute-start(bf16[128,384]{1,0:T(8,128)(2,1)S(1)} %bitcast.29), channel_id=1, source_target_pairs={{0,16},{8,24},{16,0},{24,8},{1,17},{9,25},{17,1},{25,9},{2,18},{10... | collective-permute-start | bytes 294920 | tf_op jit(solution)/shard_map/ppermute | solution.py:201
  55.7 5.9 %collective-permute-start.27 = (bf16[192,512]{1,0:T(8,128)(2,1)S(1)}, bf16[192,512]{1,0:T(8,128)(2,1)S(1)}, u32[]{:S(2)}, u32[]{:S(2)}) collective-permute-start(bf16[192,512]{1,0:T(8,128)(2,1)S(1)} %add_convert_fusion), channel_id=1, source_target_pairs={{0,8},{8,0},{16,24},{24,16},{1,9},{9,1},{17,25},{25,17},{2,10},{10... | collective-permute-start | bytes 589832 | tf_op jit(solution)/shard_map/ppermute | solution.py:198
  55.9 4.5 %collective-permute-start.24 = (bf16[64,384]{1,0:T(8,128)(2,1)S(1)}, bf16[64,384]{1,0:T(8,128)(2,1)S(1)}, u32[]{:S(2)}, u32[]{:S(2)}) collective-permute-start(bf16[64,384]{1,0:T(8,128)(2,1)S(1)} %bitcast.31), channel_id=1, source_target_pairs={{0,16},{8,24},{16,0},{24,8},{1,17},{9,25},{17,1},{25,9},{2,18},{10... | collective-permute-start | bytes 147464 | tf_op jit(solution)/shard_map/ppermute | solution.py:201
  (4 other events, 4.3 us)

commit v2 on v0

v2 whole, which is shorter than its diff:
```python
import functools
import math

import jax
import jax.numpy as jnp
from jax import lax
from jax.experimental import pallas as pl
from jax.experimental.pallas import tpu as pltpu
from jax.sharding import PartitionSpec as P


HEADS = 12
KV_HEADS = 2
HEAD_DIM = 256
GROUP = HEADS // KV_HEADS
SCALE = 1.0 / math.sqrt(HEAD_DIM)
F32 = jnp.float32
BF16 = jnp.bfloat16
VMEM = pl.BlockSpec(memory_space=pltpu.VMEM)
HBM = pl.BlockSpec(memory_space=pltpu.HBM)


def dot(a, b, contract):
    return lax.dot_general(a, b, (contract, ((), ())), preferred_element_type=F32)


NN = ((1,), (0,))
NT = ((1,), (1,))
TN = ((0,), (0,))


def call(kernel, outs, scratch, flops, operands, specs=None, out_specs=None):
    moved = sum(x.size * x.dtype.itemsize for x in operands)
    moved += sum(math.prod(o.shape) * o.dtype.itemsize for o in outs)
    return pl.pallas_call(
        kernel,
        out_shape=outs,
        in_specs=specs or [VMEM] * len(operands),
        out_specs=out_specs or [VMEM] * len(outs),
        scratch_shapes=scratch,
        cost_estimate=pl.CostEstimate(flops=flops, bytes_accessed=moved, transcendentals=0),
        compiler_params=pltpu.CompilerParams(vmem_limit_bytes=24 * 1024 * 1024),
    )(*operands)


def stack_kernel(*refs):
    each = refs[0].shape[0]
    for i, ref in enumerate(refs[:-1]):
        refs[-1][i * each : (i + 1) * each, :] = ref[...]


def prepare_kernel(q_ref, do_ref, o_ref, lse_ref, qs_ref, dos_ref, rows_ref):
    rows = q_ref.shape[0]
    lanes = lax.broadcasted_iota(jnp.int32, (rows, 128), 1)
    columns = jnp.zeros((rows, 128), F32)
    for h in range(HEADS):
        span = slice(h * HEAD_DIM, (h + 1) * HEAD_DIM)
        there = slice(h * rows, (h + 1) * rows)
        qs_ref[there, :] = q_ref[:, span]
        grad = do_ref[:, span]
        dos_ref[there, :] = grad
        total = jnp.sum(grad.astype(F32) * o_ref[:, span].astype(F32), axis=1, keepdims=True)
        columns = jnp.where(lanes == h, total, columns)
    rows_ref[:16, :] = columns.T[:16, :]
    rows_ref[16 : 16 + HEADS, :] = lse_ref[...]
    rows_ref[16 + HEADS :, :] = jnp.zeros((rows_ref.shape[0] - 16 - HEADS, rows), F32)


def place(dz, dx, each):
    other = jnp.bitwise_xor(lax.axis_index("tp"), jnp.int32(2 * dz) + dx)
    return pl.multiple_of(other * each, each)


def my_core():
    return lax.rem(lax.axis_index("sp"), 2)


def across(column):
    if column == "own":
        return 0, 0
    if column == "both":
        return 1, 1
    over_y = my_core() if column == 0 else 1 - my_core()
    return 1 - over_y, over_y


def pick_source(here_ref, there_ref, column, planes, each, src_ref):
    dx, dy = across(column)
    for b, dz in enumerate(planes):
        begin = pl.ds(place(dz, dx, each), each)
        if column == "own":
            value = here_ref[begin, :]
        elif column == "both":
            value = there_ref[begin, :]
        else:
            value = jnp.where(dy == 0, here_ref[begin, :], there_ref[begin, :])
        src_ref[b * each : (b + 1) * each, :] = value


def head_rows(ref, h):
    return jnp.concatenate([ref[pl.ds(h, 1), :], ref[pl.ds(h + 1, 1), :]], axis=1)


def chunk_kernel(columns, planes, each, mode, *refs):
    refs = list(refs)

    def take(n):
        out = refs[:n]
        del refs[:n]
        return out

    blocks = [take(3), take(3)]
    wk_ref, wv_ref, piece = take(3)
    source = take(2) if mode == "merge" else None
    old = take(3) if mode == "merge" else None
    given = take(2) if mode == "rest" else None
    ds_ref = take(1)[0]
    outs = take({"keep": 2, "merge": 3, "rest": 1}[mode])
    p_ref, dkv_ref, src_ref = refs
    width = wk_ref.shape[1]
    rows = blocks[0][0].shape[0] // HEADS
    stacked = GROUP * rows
    step = 2 * rows
    if given is not None:
        for x, g in zip(given, (1 - my_core(), my_core())):
            dkv_ref[:, pl.ds(pl.multiple_of(width + g * HEAD_DIM, HEAD_DIM), HEAD_DIM)] = x[...]
    for g in range(KV_HEADS):
        cols = slice(g * HEAD_DIM, (g + 1) * HEAD_DIM)
        vcols = slice(width + g * HEAD_DIM, width + (g + 1) * HEAD_DIM)
        mine = slice(g * stacked, (g + 1) * stacked)
        k, v = piece[:, cols], piece[:, vcols]
        dk = dv = 0.0
        for t, (q_ref, do_ref, rows_ref) in enumerate(blocks):
            base = t * HEADS * rows
            for n in range(stacked // step):
                at = slice(g * stacked + n * step, g * stacked + (n + 1) * step)
                h = g * GROUP + 2 * n
                probs = jnp.exp(dot(k, q_ref[at, :], NT) * SCALE - head_rows(rows_ref, 16 + h))
                if given is None:
                    p_ref[:, t * stacked + n * step : t * stacked + (n + 1) * step] = probs.astype(BF16)
                dprob = dot(v, do_ref[at, :], NT)
                grads = probs * (dprob - head_rows(rows_ref, h))
                ds_ref[:, base + at.start : base + at.stop] = grads.astype(BF16)
            dk += dot(ds_ref[:, base + mine.start : base + mine.stop], q_ref[mine, :], NN)
            if given is None:
                dv += dot(p_ref[:, t * stacked : (t + 1) * stacked], do_ref[mine, :], NN)
        dkv_ref[:, cols] = (dk * SCALE).astype(BF16)
        if given is None:
            dkv_ref[:, vcols] = dv.astype(BF16)
    part = dot(dkv_ref[:, :width], wk_ref[...], NT) + dot(dkv_ref[:, width:], wv_ref[...], NT)
    if mode == "rest":
        outs[0][...] = part.astype(BF16)
        return
    if mode == "keep":
        outs[0][...] = part
        outs[1][...] = dkv_ref[:, width:]
        return
    other_part, *gradients = old
    x_ref, y_ref, total_ref = outs
    dx, _ = across(columns[2])
    x_ref[...] = jnp.where(dx == 1, part, other_part[...])
    y_ref[...] = jnp.where(dx == 1, other_part[...], part).astype(BF16)
    total = None
    for column, dv_ref in zip(columns, (*gradients, dkv_ref.at[:, width:])):
        pick_source(*source, column, planes, each, src_ref)
        term = dot(src_ref[...], dv_ref[...], TN)
        total = term if total is None else total + term
    total_ref[...] = total


def value_kernel(column, planes, each, mine, *refs):
    blocks, refs = [refs[:3], refs[3:6]], refs[6:]
    piece, here_ref, there_ref, old_ref, dv_ref, out_ref, p_ref, src_ref = refs
    rows = blocks[0][0].shape[0] // HEADS
    stacked = GROUP * rows
    step = 2 * rows
    g = my_core() if mine else 1 - my_core()
    pick_source(here_ref, there_ref, column, planes, each, src_ref)
    cols = pl.ds(pl.multiple_of(g * HEAD_DIM, HEAD_DIM), HEAD_DIM)
    all_rows = pl.ds(pl.multiple_of(g * stacked, stacked), stacked)
    k = piece[:, cols]
    dv = 0.0
    for t, (q_ref, do_ref, rows_ref) in enumerate(blocks):
        for n in range(stacked // step):
            at = pl.ds(pl.multiple_of(g * stacked + n * step, step), step)
            lse = head_rows(rows_ref, 16 + g * GROUP + 2 * n)
            probs = jnp.exp(dot(k, q_ref[at, :], NT) * SCALE - lse)
            p_ref[:, t * stacked + n * step : t * stacked + (n + 1) * step] = probs.astype(BF16)
        dv += dot(p_ref[:, t * stacked : (t + 1) * stacked], do_ref[all_rows, :], NN)
    dv_ref[...] = dv.astype(BF16)
    out_ref[...] = (old_ref[:, cols] + dot(src_ref[...], dv_ref[...], TN)).astype(out_ref.dtype)


def target_kernel(g, n, last, *refs):
    refs = list(refs)
    wq_hbm = refs.pop(0)
    old_ref = refs.pop(0) if last else None
    ds_refs, pieces = refs[:n], refs[n : 2 * n]
    outs = refs[2 * n : -4]
    kt_ref, dq_ref, wq_ref, sem = refs[-4:]
    span = GROUP * HEAD_DIM
    copy = pltpu.make_async_copy(wq_hbm.at[:, g * span : (g + 1) * span], wq_ref, sem)
    copy.start()
    rows = ds_refs[0].shape[1] // (2 * HEADS)
    keys = jnp.concatenate([x[:, g * HEAD_DIM : (g + 1) * HEAD_DIM] for x in pieces], axis=0)
    kt_ref[...] = keys.T
    for i in range(GROUP):
        at = [(t * HEADS + g * GROUP + i) * rows for t in range(2)]
        grads = [jnp.concatenate([ds[:, x : x + rows] for x in at], axis=1) for ds in ds_refs]
        dq = dot(kt_ref[...], jnp.concatenate(grads, axis=0), NN) * SCALE
        dq_ref[i * HEAD_DIM : (i + 1) * HEAD_DIM, :] = dq.astype(BF16)
    copy.wait()
    total = dot(wq_ref[...], dq_ref[...], NN)
    if not last:
        outs[0][...] = total
        return
    total += old_ref[...]
    for t in range(2):
        outs[t][...] = total[:, t * rows : (t + 1) * rows].T


def finish_kernel(planes, each, mine_ref, other_ref, near0_ref, near1_ref, y0_ref, y1_ref, *refs):
    source_hbm, value_hbm, source_ref, value_ref, sem = refs
    half = mine_ref.shape[1]
    copies = []
    for i, (ref, which) in enumerate(((mine_ref, my_core()), (other_ref, 1 - my_core()))):
        value_ref[i] = ref[...].astype(F32)
        columns = pl.ds(pl.multiple_of(which * half, half), half)
        copies.append(pltpu.make_async_copy(value_ref.at[i], value_hbm.at[:, columns], sem.at[i]))
        copies[-1].start()
    for dx, (near_ref, y_ref) in enumerate(((near0_ref, y0_ref), (near1_ref, y1_ref))):
        for b, dz in enumerate(planes):
            span = slice(b * each, (b + 1) * each)
            value = near_ref[span, :] + y_ref[span, :].astype(F32)
            source_ref[pl.ds(place(dz, dx, each), each), :] = value.astype(BF16)
    copies.append(pltpu.make_async_copy(source_ref, source_hbm, sem.at[2]))
    copies[-1].start()
    for copy in copies:
        copy.wait()


def gathered(n_sp, n_tp, queries, attn_out, log_norm, cotangent, keys, values, source, w_query, w_key, w_value):
    rows = queries.shape[0]
    each, width = keys.shape
    cols = w_key.shape[0]
    shape = jax.ShapeDtypeStruct
    everyone = range(n_sp * n_tp)

    def across(i, first):
        return i ^ 1 if i // n_tp % 2 == first else i ^ (2 * n_tp)

    rings = {
        "core": ("sp", [(i, i ^ 1) for i in range(n_sp)]),
        "y": ("sp", [(i, i ^ 2) for i in range(n_sp)]),
        "xy": (("sp", "tp"), [(i, across(i, 0)) for i in everyone]),
        "yx": (("sp", "tp"), [(i, across(i, 1)) for i in everyone]),
    }
    planes = range(n_tp // 2)
    for dz in planes[1:]:
        rings[f"z{dz}"] = ("tp", [(i, i ^ (2 * dz)) for i in range(n_tp)])

    def move(ring, a):
        axis, pairs = rings[ring]
        return lax.ppermute(a, axis, pairs)

    own = jnp.maximum(
        lax.pad(keys, jnp.asarray(-jnp.inf, keys.dtype), ((0, 0, 0), (0, width, 0))),
        lax.pad(values, jnp.asarray(-jnp.inf, values.dtype), ((0, 0, 0), (width, 0, 0))),
    )
    (held,) = call(stack_kernel, [shape(own.shape, BF16)], [], 5 * 10**9, (own,))
    qs, dos, head = call(
        prepare_kernel,
        [shape((HEADS * rows, HEAD_DIM), BF16)] * 2 + [shape((32, rows), F32)],
        [],
        10 * queries.size,
        (queries, cotangent, attn_out, log_norm.T),
    )
    targets = [qs, dos, head]
    targets += [move("core", a) for a in (qs, dos, head)]

    (column,) = call(
        stack_kernel,
        [shape((len(planes) * each, 2 * width), BF16)],
        [],
        10**6,
        [held] + [move(f"z{dz}", own) for dz in planes[1:]],
    )
    near_a = move("xy", column)
    near_b = move("yx", column)
    diagonal = move("yx", near_a)
    pieces = (column, near_a, near_b, diagonal)
    columns = ("own", 0, 1, "both")
    src = (source, move("y", source))

    size = column.shape[0]
    flops = 4 * size * rows * HEADS * HEAD_DIM * 4 + 2 * size * cols * width * 3
    part_f32, part_bf16 = shape((size, cols), F32), shape((size, cols), BF16)

    def chunk(c, mode, outs, extra):
        return call(
            functools.partial(chunk_kernel, columns[: c + 1], planes, each, mode),
            [shape((size, 2 * HEADS * rows), BF16)] + outs,
            [
                pltpu.VMEM((size, 2 * GROUP * rows), BF16),
                pltpu.VMEM((size, 2 * width), BF16),
                pltpu.VMEM((size, cols), BF16),
            ],
            flops,
            [*targets, w_key, w_value, pieces[c], *extra],
        )

    grads = shape((size, width), BF16)
    ds0, near0, dv0 = chunk(0, "keep", [part_f32, grads], ())
    ds1, part1, dv1 = chunk(1, "keep", [part_f32, grads], ())
    ds2, near1, far0, total = chunk(
        2, "merge", [part_f32, part_bf16, shape((cols, width), F32)], (*src, part1, dv0, dv1)
    )
    y0 = move("y", far0)
    given, sides = [], []
    for i, kind in enumerate((BF16, F32)):
        dv, side = call(
            functools.partial(value_kernel, columns[3], planes, each, i == 1),
            [shape((size, HEAD_DIM), BF16), shape((cols, HEAD_DIM), kind)],
            [pltpu.VMEM((size, 2 * GROUP * rows), BF16), pltpu.VMEM((size, cols), BF16)],
            flops // 5,
            [*targets, diagonal, *src, total],
        )
        given.append(dv)
        sides.append(side)
    ds3, far1 = chunk(3, "rest", [part_bf16], given)
    y1 = move("y", far1)

    wv = (sides[1] + move("core", sides[0]).astype(F32)).astype(BF16)
    wv = (wv.astype(F32) + move("y", wv).astype(F32)).astype(BF16)
    wv_other = move("core", wv)

    all_ds = (ds0, ds1, ds2, ds3)
    terms = None
    for g in range(KV_HEADS):
        last = g == KV_HEADS - 1
        terms = call(
            functools.partial(target_kernel, g, len(all_ds), last),
            [shape((rows, cols), F32)] * 2 if last else [shape((cols, 2 * rows), F32)],
            [
                pltpu.VMEM((HEAD_DIM, size * len(pieces)), BF16),
                pltpu.VMEM((GROUP * HEAD_DIM, 2 * rows), BF16),
                pltpu.VMEM((cols, GROUP * HEAD_DIM), BF16),
                pltpu.SemaphoreType.DMA,
            ],
            4 * rows * GROUP * HEAD_DIM * (size * len(pieces) + cols),
            (w_query, *(terms if last else ()), *all_ds, *pieces),
            specs=[HBM] + [VMEM] * (2 * len(pieces) + last),
        )
    d_target = (terms[0] + move("core", terms[1])).astype(BF16)
    d_source, d_wvalue = call(
        functools.partial(finish_kernel, planes, each),
        [shape((source.shape[0], cols), BF16), shape((cols, width), F32)],
        [
            pltpu.VMEM((source.shape[0], cols), BF16),
            pltpu.VMEM((2, cols, HEAD_DIM), F32),
            pltpu.SemaphoreType.DMA((3,)),
        ],
        2 * source.size,
        (wv, wv_other, near0, near1, y0, y1),
        out_specs=[HBM] * 2,
    )
    return d_target, d_source, d_wvalue


def sharded(queries, attn_out, log_norm, cotangent, keys, values, source, w_query, w_key, w_value):
    rows = queries.shape[0]
    near_keys, near_values = (
        lax.all_gather(keys, "sp", axis=0, tiled=True),
        lax.all_gather(values, "sp", axis=0, tiled=True),
    )
    span = near_keys.shape[0]
    q4 = queries.reshape(rows, KV_HEADS, GROUP, HEAD_DIM)
    g4 = cotangent.reshape(rows, KV_HEADS, GROUP, HEAD_DIM)
    o4 = attn_out.reshape(rows, KV_HEADS, GROUP, HEAD_DIM)
    k3 = near_keys.reshape(span, KV_HEADS, HEAD_DIM)
    v3 = near_values.reshape(span, KV_HEADS, HEAD_DIM)
    delta = jnp.sum(g4.astype(F32) * o4.astype(F32), axis=3)
    delta = jnp.transpose(delta, (1, 2, 0))[..., None]
    lse = jnp.transpose(log_norm.reshape(rows, KV_HEADS, GROUP), (1, 2, 0))[..., None]
    scores = jnp.einsum("znjk,wnk->njzw", q4, k3, preferred_element_type=F32) * SCALE
    probs = jnp.exp(scores - lse)
    probs16 = probs.astype(BF16)
    dprob = jnp.einsum("znjk,wnk->njzw", g4, v3, preferred_element_type=F32)
    dscore = (probs * (dprob - delta)).astype(BF16)
    dq = jnp.einsum("wohn,nwb->hwob", dscore, k3, preferred_element_type=F32) * SCALE
    dk = jnp.einsum("nkjv,jnka->vna", dscore, q4, preferred_element_type=F32) * SCALE
    dv = jnp.einsum("nkjv,jnka->vna", probs16, g4, preferred_element_type=F32)
    own = [
        lax.psum_scatter(a.reshape(span, -1).astype(BF16), "sp", scatter_dimension=0, tiled=True)
        for a in (dk, dv)
    ]
    group = lax.all_gather(jnp.concatenate(own, axis=1), "tp", axis=0, tiled=True)
    weights = jnp.concatenate([w_key, w_value], axis=1)
    d_source = dot(group, weights, NT).astype(BF16)
    term = dot(source, group[:, w_value.shape[1] :], TN)
    d_wvalue = lax.psum(term.astype(BF16), "sp").astype(F32)
    dq16 = lax.psum(dq.reshape(rows, -1), "tp").astype(BF16)
    d_target = dot(dq16, w_query, NT).astype(BF16)
    return d_target, d_source, d_wvalue


def solution(mesh):
    n_sp, n_tp = mesh.shape["sp"], mesh.shape["tp"]
    near = (n_sp, n_tp) == (4, 8)

    def shards(*args):
        if not near:
            return sharded(*args)
        return gathered(n_sp, n_tp, *args)

    in_specs = (
        P("sp", None),
        P("sp", None),
        P("sp", None),
        P("sp", None),
        P(("sp", "tp"), None),
        P(("sp", "tp"), None),
        P("sp", "tp"),
        P("tp", None),
        P("tp", None),
        P("tp", None),
    )
    out_specs = (P("sp", "tp"), P("sp", "tp"), P("tp", None))
    return jax.shard_map(shards, mesh=mesh, in_specs=in_specs, out_specs=out_specs, check_vma=False)
```

time: 198 us -> 46.7 us (0.24)
  blocking collectives: 125 us -> 0 us
  waiting for transfers between devices: 31.6 us -> 13 us
  starting transfers between devices: 0.12 us -> 14.4 us
  Pallas kernels: 0 us -> 13.3 us
  between operations: 13.9 us -> 0.84 us
  local copies, waits for them, and re-layouts: 15.6 us -> 4.12 us
  matrix products: 8.94 us -> 0 us
    psum x1 -> x0, blocking collectives: 80.8 us -> none  [shards(): dq16 = lax.psum(query_gradient_piece, 'tp').astype(jnp.bfloat16)]
    all_gather x3 -> x0, blocking collectives: 43.8 us -> none  [the longest x1 31.5 us: shards(): group = lax.all_gather(stacked, 'tp', axis=0, tiled=True)]
    psum x1 -> x0, waiting for transfers between devices: 31.5 us -> none  [shards(): lax.psum(weight_term.astype(jnp.bfloat16), 'sp').astype(jnp.float32)]
    ppermute x0 -> x16, starting transfers between devices: none -> 14.4 us  [move(): return lax.ppermute(a, axis, pairs)]
    pallas_call x0 -> x12, Pallas kernels: none -> 13.3 us  [call(): pl.pallas_call(kernel, out_shape=outs, in_specs=specs or [VMEM] * len(ope...]
    ppermute x0 -> x16, waiting for transfers between devices: none -> 13 us  [move(): return lax.ppermute(a, axis, pairs)]
    dot_general x8 -> x0, matrix products: 8.94 us -> none  [the longest x1 2.25 us: shards(): lax.dot_general(group, weights, (((1,), (1,)), ((), ())), preferred_eleme...]
    unnamed x24 -> x20, local copies, waits for them, and re-layouts: 10.6 us -> 4.12 us
  transfers between devices with their start and end apart: 3 -> 16, of which waited for: 1 -> 7; matrix products, arithmetic and copies ran while one was open for 7% -> 2% of each run, Pallas kernels for 0% -> 24%
where the time goes in v2:
time: 46.7 us; the launch traced here: 46.4 us
  starting transfers between devices  14.4 us (31%)
  Pallas kernels  13.3 us (28%)
  waiting for transfers between devices  13 us (28%)
  local copies, waits for them, and re-layouts  4.12 us (9%)
  between operations  0.84 us (2%)
  other arithmetic  0.76 us (2%)
    ppermute x16, starting transfers between devices, move(): return lax.ppermute(a, axis, pairs)  14.4 us
    pallas_call x12, Pallas kernels, call(): pl.pallas_call(kernel, out_shape=outs, in_specs=specs or [VMEM] * len(ope...  13.3 us
    ppermute x16, waiting for transfers between devices, move(): return lax.ppermute(a, axis, pairs)  13 us
    unnamed x20, local copies, waits for them, and re-layouts  4.12 us
  transfers between devices with their start and end apart: 16, of which 7 were waited for; matrix products, arithmetic and copies ran while one was open for 2% of the time, Pallas kernels for 24%

profile of v2, /device:TPU:0, one launch (start us, length us, event | category | flops | bytes accessed | tf_op | source)
XLA Modules:
  0.0 46.4 jit_solution(4798363697510893736)
XLA Ops:
  0.6 1.1 %copy-done.4 = bf16[128,3072]{1,0:T(8,128)(2,1)S(1)} copy-done((bf16[128,3072]{1,0:T(8,128)(2,1)S(1)}, bf16[128,3072]{1,0:T(8,128)(2,1)}, u32[]{:S(2)}) %copy-start.4) | copy-done | bytes 786456
  1.8 1.1 %copy-done.5 = bf16[128,3072]{1,0:T(8,128)(2,1)S(1)} copy-done((bf16[128,3072]{1,0:T(8,128)(2,1)S(1)}, bf16[128,3072]{1,0:T(8,128)(2,1)}, u32[]{:S(2)}) %copy-start.5) | copy-done | bytes 786456
  2.9 1.1 %copy-done.6 = bf16[128,3072]{1,0:T(8,128)(2,1)S(1)} copy-done((bf16[128,3072]{1,0:T(8,128)(2,1)S(1)}, bf16[128,3072]{1,0:T(8,128)(2,1)}, u32[]{:S(2)}) %copy-start.6) | copy-done | bytes 786456
  4.0 0.7 %copy-done.7 = f32[128,12]{0,1:T(8,128)S(1)} copy-done((f32[128,12]{0,1:T(8,128)S(1)}, f32[128,12]{0,1:T(8,128)}, u32[]{:S(2)}) %copy-start.7) | copy-done | bytes 6168
  4.7 0.3 shard_map.121
  5.1 0.5 %collective-permute-start = (bf16[1536,256]{1,0:T(8,128)(2,1)S(1)}, bf16[1536,256]{1,0:T(8,128)(2,1)S(1)}, u32[]{:S(2)}, u32[]{:S(2)}) collective-permute-start(bf16[1536,256]{1,0:T(8,128)(2,1)S(1)} %get-tuple-element.26.refs_0_), channel_id=1, source_target_pairs={{0,8},{8,0},{16,24},{24,16},{1,9},{9,1},{17,25},{25,17},{2,10},{10... | collective-permute-start | bytes 2359304 | tf_op jit(solution)/shard_map/ppermute | solution.py:264
  5.7 5.1 %collective-permute-start.5 = (bf16[32,1024]{1,0:T(8,128)(2,1)S(1)}, bf16[32,1024]{1,0:T(8,128)(2,1)S(1)}, u32[]{:S(2)}, u32[]{:S(2)}) collective-permute-start(bf16[32,1024]{1,0:T(8,128)(2,1)S(1)} %pad_maximum_fusion.refs_0_), channel_id=1, source_target_pairs={{0,6},{1,7},{2,4},{3,5},{4,2},{5,3},{6,0},{7,1},{8,14},{9,15},{10,... | collective-permute-start | bytes 196616 | tf_op jit(solution)/shard_map/ppermute | solution.py:264
  10.8 0.6 %collective-permute-start.3 = (bf16[32,1024]{1,0:T(8,128)(2,1)S(1)}, bf16[32,1024]{1,0:T(8,128)(2,1)S(1)}, u32[]{:S(2)}, u32[]{:S(2)}) collective-permute-start(bf16[32,1024]{1,0:T(8,128)(2,1)S(1)} %pad_maximum_fusion.refs_0_), channel_id=1, source_target_pairs={{0,2},{1,3},{2,0},{3,1},{4,6},{5,7},{6,4},{7,5},{8,10},{9,11},{10,... | collective-permute-start | bytes 196616 | tf_op jit(solution)/shard_map/ppermute | solution.py:264
  11.4 1.9 %collective-permute-done.5.refs_3_ = bf16[32,1024]{1,0:T(8,128)(2,1)S(1)} collective-permute-done((bf16[32,1024]{1,0:T(8,128)(2,1)S(1)}, bf16[32,1024]{1,0:T(8,128)(2,1)S(1)}, u32[]{:S(2)}, u32[]{:S(2)}) %collective-permute-start.5) | collective-permute-done | bytes 65568 | tf_op jit(solution)/shard_map/ppermute | solution.py:264
  13.3 3.3 %collective-permute-done.4.refs_2_ = bf16[32,1024]{1,0:T(8,128)(2,1)S(1)} collective-permute-done((bf16[32,1024]{1,0:T(8,128)(2,1)S(1)}, bf16[32,1024]{1,0:T(8,128)(2,1)S(1)}, u32[]{:S(2)}, u32[]{:S(2)}) %collective-permute-start.4) | collective-permute-done | bytes 65568 | tf_op jit(solution)/shard_map/ppermute | solution.py:264
  16.7 1.6 %collective-permute-start.6 = (bf16[128,1024]{1,0:T(8,128)(2,1)S(1)}, bf16[128,1024]{1,0:T(8,128)(2,1)S(1)}, u32[]{:S(2)}, u32[]{:S(2)}) collective-permute-start(bf16[128,1024]{1,0:T(8,128)(2,1)S(1)} %shard_map.123.refs_8_.refs_5_.refs_6_), channel_id=1, source_target_pairs={{0,1},{1,0},{2,3},{3,2},{4,5},{5,4},{6,7},{7,6},{8,24},{9,25},{10,... | collective-permute-start | bytes 786440 | tf_op jit(solution)/shard_map/ppermute | solution.py:264
  18.2 1.5 %collective-permute-start.7 = (bf16[128,1024]{1,0:T(8,128)(2,1)S(1)}, bf16[128,1024]{1,0:T(8,128)(2,1)S(1)}, u32[]{:S(2)}, u32[]{:S(2)}) collective-permute-start(bf16[128,1024]{1,0:T(8,128)(2,1)S(1)} %shard_map.123.refs_8_.refs_5_.refs_6_), channel_id=1, source_target_pairs={{0,16},{1,17},{2,18},{3,19},{4,20},{5,21},{6,22},{7,23},{8,9},{9,8... | collective-permute-start | bytes 786440 | tf_op jit(solution)/shard_map/ppermute | solution.py:264
  19.7 1.2 %collective-permute-done.2.refs_5_ = f32[32,128]{1,0:T(8,128)S(1)} collective-permute-done((f32[32,128]{1,0:T(8,128)S(1)}, f32[32,128]{1,0:T(8,128)S(1)}, u32[]{:S(2)}, u32[]{:S(2)}) %collective-permute-start.2) | collective-permute-done | bytes 16416 | tf_op jit(solution)/shard_map/ppermute | solution.py:264
  20.9 0.5 %collective-permute-start.8 = (bf16[256,384]{1,0:T(8,128)(2,1)S(1)}, bf16[256,384]{1,0:T(8,128)(2,1)S(1)}, u32[]{:S(2)}, u32[]{:S(2)}) collective-permute-start(bf16[256,384]{1,0:T(8,128)(2,1)S(1)} %copy-done.3), channel_id=1, source_target_pairs={{0,16},{8,24},{16,0},{24,8},{1,17},{9,25},{17,1},{25,9},{2,18},{10... | collective-permute-start | bytes 589832 | tf_op jit(solution)/shard_map/ppermute | solution.py:264
  21.4 4.5 %collective-permute-done.6.refs_8_.refs_6_.refs_7_ = bf16[128,1024]{1,0:T(8,128)(2,1)S(1)} collective-permute-done((bf16[128,1024]{1,0:T(8,128)(2,1)S(1)}, bf16[128,1024]{1,0:T(8,128)(2,1)S(1)}, u32[]{:S(2)}, u32[]{:S(2)}) %collective-permute-start.6) | collective-permute-done | bytes 262176 | tf_op jit(solution)/shard_map/ppermute | solution.py:264
  25.9 0.4 collective-permute-start.9
  26.4 1.9 %shard_map.125 = (bf16[128,3072]{1,0:T(8,128)(2,1)S(1)}, f32[128,384]{1,0:T(8,128)S(1)}, bf16[128,512]{1,0:T(8,128)(2,1)S(1)}) custom-call(bf16[1536,256]{1,0:T(8,128)(2,1)S(1)} %get-tuple-element.26.refs_0_, bf16[1536,256]{1,0:T(8,128)(2,1)S(1)} %get-tuple-element.27.refs_1_, f32[32,128]{1,0:T(8,128)S(1)} %get-tuple-element.28.refs_2_, ...), custom_call_target="tpu_custom_call" | custom-call | flops 956301312 | bytes 5341184 | tf_op jit(solution)/shard_map/pallas_call | solution.py:35
  28.3 1.9 %shard_map.124 = (bf16[128,3072]{1,0:T(8,128)(2,1)S(1)}, f32[128,384]{1,0:T(8,128)S(1)}, bf16[128,512]{1,0:T(8,128)(2,1)S(1)}) custom-call(bf16[1536,256]{1,0:T(8,128)(2,1)S(1)} %get-tuple-element.26.refs_0_, bf16[1536,256]{1,0:T(8,128)(2,1)S(1)} %get-tuple-element.27.refs_1_, f32[32,128]{1,0:T(8,128)S(1)} %get-tuple-element.28.refs_2_, ...), custom_call_target="tpu_custom_call" | custom-call | flops 956301312 | bytes 5341184 | tf_op jit(solution)/shard_map/pallas_call | solution.py:35
  30.2 2.2 %shard_map.126 = (bf16[128,3072]{1,0:T(8,128)(2,1)S(1)}, f32[128,384]{1,0:T(8,128)S(1)}, bf16[128,384]{1,0:T(8,128)(2,1)S(1)}, f32[384,512]{1,0:T(8,128)S(1)}) custom-call(bf16[1536,256]{1,0:T(8,128)(2,1)S(1)} %get-tuple-element.26.refs_0_, bf16[1536,256]{1,0:T(8,128)(2,1)S(1)} %get-tuple-element.27.refs_1_, f32[32,128]{1,0:T(8,128)S(1)} %get-tuple-element.28.refs_2_, ...), custom_call_target="tpu_custom_call" | custom-call | flops 956301312 | bytes 6946816 | tf_op jit(solution)/shard_map/pallas_call | solution.py:35
  32.4 0.9 %shard_map.127 = (bf16[128,256]{1,0:T(8,128)(2,1)S(1)}, bf16[384,256]{1,0:T(8,128)(2,1)S(1)}) custom-call(bf16[1536,256]{1,0:T(8,128)(2,1)S(1)} %get-tuple-element.26.refs_0_, bf16[1536,256]{1,0:T(8,128)(2,1)S(1)} %get-tuple-element.27.refs_1_, f32[32,128]{1,0:T(8,128)S(1)} %get-tuple-element.28.refs_2_, bf16[1536,256]{1,0:T(8,128)(2,1)S(1)} %collective-permute-done.refs_3_, ...), custom_call_target="tpu_custom_call" | custom-call | flops 191260256 | bytes 4882432 | tf_op jit(solution)/shard_map/pallas_call | solution.py:35
  33.4 1.6 %collective-permute-start.14 = (bf16[128,384]{1,0:T(8,128)(2,1)S(1)}, bf16[128,384]{1,0:T(8,128)(2,1)S(1)}, u32[]{:S(2)}, u32[]{:S(2)}) collective-permute-start(bf16[128,384]{1,0:T(8,128)(2,1)S(1)} %get-tuple-element.45), channel_id=1, source_target_pairs={{0,16},{8,24},{16,0},{24,8},{1,17},{9,25},{17,1},{25,9},{2,18},{10... | collective-permute-start | bytes 294920 | tf_op jit(solution)/shard_map/ppermute | solution.py:264
  35.1 0.9 %shard_map.128 = (bf16[128,256]{1,0:T(8,128)(2,1)S(1)}, f32[384,256]{1,0:T(8,128)S(1)}) custom-call(bf16[1536,256]{1,0:T(8,128)(2,1)S(1)} %get-tuple-element.26.refs_0_, bf16[1536,256]{1,0:T(8,128)(2,1)S(1)} %get-tuple-element.27.refs_1_, f32[32,128]{1,0:T(8,128)S(1)} %get-tuple-element.28.refs_2_, bf16[1536,256]{1,0:T(8,128)(2,1)S(1)} %collective-permute-done.refs_3_, ...), custom_call_target="tpu_custom_call" | custom-call | flops 191260256 | bytes 5079040 | tf_op jit(solution)/shard_map/pallas_call | solution.py:35
  36.0 0.5 %collective-permute-start.12 = (bf16[384,256]{1,0:T(8,128)(2,1)S(1)}, bf16[384,256]{1,0:T(8,128)(2,1)S(1)}, u32[]{:S(2)}, u32[]{:S(2)}) collective-permute-start(bf16[384,256]{1,0:T(8,128)(2,1)S(1)} %add_convert_fusion.1), channel_id=1, source_target_pairs={{0,16},{8,24},{16,0},{24,8},{1,17},{9,25},{17,1},{25,9},{2,18},{10... | collective-permute-start | bytes 589832 | tf_op jit(solution)/shard_map/ppermute | solution.py:264
  36.6 1.7 %shard_map.129 = (bf16[128,3072]{1,0:T(8,128)(2,1)S(1)}, bf16[128,384]{1,0:T(8,128)(2,1)S(1)}) custom-call(bf16[1536,256]{1,0:T(8,128)(2,1)S(1)} %get-tuple-element.26.refs_0_, bf16[1536,256]{1,0:T(8,128)(2,1)S(1)} %get-tuple-element.27.refs_1_, f32[32,128]{1,0:T(8,128)S(1)} %get-tuple-element.28.refs_2_, ...), custom_call_target="tpu_custom_call" | custom-call | flops 956301312 | bytes 5242880 | tf_op jit(solution)/shard_map/pallas_call | solution.py:35
  38.3 1.6 %collective-permute-start.15 = (bf16[128,384]{1,0:T(8,128)(2,1)S(1)}, bf16[128,384]{1,0:T(8,128)(2,1)S(1)}, u32[]{:S(2)}, u32[]{:S(2)}) collective-permute-start(bf16[128,384]{1,0:T(8,128)(2,1)S(1)} %get-tuple-element.46), channel_id=1, source_target_pairs={{0,16},{8,24},{16,0},{24,8},{1,17},{9,25},{17,1},{25,9},{2,18},{10... | collective-permute-start | bytes 294920 | tf_op jit(solution)/shard_map/ppermute | solution.py:264
  39.9 1.2 %shard_map.130.refs_1_ = f32[384,256]{1,0:T(8,128)S(1)} custom-call(bf16[384,3072]{1,0:T(8,128)(2,1)S(1)} %copy-done, bf16[128,3072]{1,0:T(8,128)(2,1)S(1)} %get-tuple-element.29.refs_1_.refs_2_, bf16[128,3072]{1,0:T(8,128)(2,1)S(1)} %get-tuple-element.30.refs_2_.refs_3_, bf16[128,3072]{1,0:T(8,128)(2,1)S(1)} %get-tuple-element.34.refs_3_.refs_4_, ...), custom_call_target="tpu_custom_call" | custom-call | flops 704643072 | bytes 6946816 | tf_op jit(solution)/shard_map/pallas_call | solution.py:35
  41.1 1.3 %shard_map.131 = (f32[128,384]{1,0:T(8,128)S(1)}, f32[128,384]{1,0:T(8,128)S(1)}) custom-call(bf16[384,3072]{1,0:T(8,128)(2,1)S(1)} %copy-done, f32[384,256]{1,0:T(8,128)S(1)} %shard_map.130.refs_1_, bf16[128,3072]{1,0:T(8,128)(2,1)S(1)} %get-tuple-element.29.refs_1_.refs_2_, bf16[128,3072]{1,0:T(8,128)(2,1)S(1)} %get-tuple-element.30.refs_2_.refs_3_, ...), custom_call_target="tpu_custom_call" | custom-call | flops 704643072 | bytes 7340032 | tf_op jit(solution)/shard_map/pallas_call | solution.py:35
  42.5 1.4 %collective-permute-done.12 = bf16[384,256]{1,0:T(8,128)(2,1)S(1)} collective-permute-done((bf16[384,256]{1,0:T(8,128)(2,1)S(1)}, bf16[384,256]{1,0:T(8,128)(2,1)S(1)}, u32[]{:S(2)}, u32[]{:S(2)}) %collective-permute-start.12) | collective-permute-done | bytes 196640 | tf_op jit(solution)/shard_map/ppermute | solution.py:264
  44.0 0.7 %add_convert_fusion.2 = bf16[128,384]{1,0:T(8,128)(2,1)} fusion(f32[128,384]{1,0:T(8,128)S(1)} %get-tuple-element.39, f32[128,384]{1,0:T(8,128)S(1)} %collective-permute-done.10), kind=kLoop, calls=%fused_computation.2 | loop fusion | flops 98304 | bytes 491520 | tf_op jit(solution)/shard_map/convert_element_type | solution.py:354
  44.7 0.5 %collective-permute-done.15.y1_ref = bf16[128,384]{1,0:T(8,128)(2,1)S(1)} collective-permute-done((bf16[128,384]{1,0:T(8,128)(2,1)S(1)}, bf16[128,384]{1,0:T(8,128)(2,1)S(1)}, u32[]{:S(2)}, u32[]{:S(2)}) %collective-permute-start.15) | collective-permute-done | bytes 98336 | tf_op jit(solution)/shard_map/ppermute | solution.py:264
  45.2 0.3 collective-permute-done.13.other_ref
  45.4 1.0 %shard_map.132 = (bf16[256,384]{1,0:T(8,128)(2,1)}, f32[384,512]{1,0:T(8,128)}) custom-call(bf16[384,256]{1,0:T(8,128)(2,1)S(1)} %add_convert_fusion.mine_ref, bf16[384,256]{1,0:T(8,128)(2,1)S(1)} %collective-permute-done.13.other_ref, f32[128,384]{1,0:T(8,128)S(1)} %get-tuple-element.43.near0_ref, f32[128,384]{1,0:T(8,128)S(1)} %get-tuple-element.44.near1_ref, ...), custom_call_target="tpu_custom_call" | custom-call | flops 196608 | bytes 1966080 | tf_op jit(solution)/shard_map/pallas_call | solution.py:35
  (36 shorter events, 0.5 us)
Async XLA Ops:
  0.6 1.1 %copy-start.4 = (bf16[128,3072]{1,0:T(8,128)(2,1)S(1)}, bf16[128,3072]{1,0:T(8,128)(2,1)}, u32[]{:S(2)}) copy-start(bf16[128,3072]{1,0:T(8,128)(2,1)} %q_ref.1) | copy-start | bytes 2359300
  1.8 1.1 %copy-start.5 = (bf16[128,3072]{1,0:T(8,128)(2,1)S(1)}, bf16[128,3072]{1,0:T(8,128)(2,1)}, u32[]{:S(2)}) copy-start(bf16[128,3072]{1,0:T(8,128)(2,1)} %do_ref.1) | copy-start | bytes 2359300
  2.9 1.1 %copy-start.6 = (bf16[128,3072]{1,0:T(8,128)(2,1)S(1)}, bf16[128,3072]{1,0:T(8,128)(2,1)}, u32[]{:S(2)}) copy-start(bf16[128,3072]{1,0:T(8,128)(2,1)} %o_ref.1) | copy-start | bytes 2359300
  4.0 0.7 %copy-start.7 = (f32[128,12]{0,1:T(8,128)S(1)}, f32[128,12]{0,1:T(8,128)}, u32[]{:S(2)}) copy-start(f32[128,12]{0,1:T(8,128)} %param.12) | copy-start | bytes 18436
  4.7 0.9 %copy-start.8 = (bf16[32,512]{1,0:T(8,128)(2,1)S(1)}, bf16[32,512]{1,0:T(8,128)(2,1)}, u32[]{:S(2)}) copy-start(bf16[32,512]{1,0:T(8,128)(2,1)} %param.15) | copy-start | bytes 98308
  4.7 0.9 %copy-start.9 = (bf16[32,512]{1,0:T(8,128)(2,1)S(1)}, bf16[32,512]{1,0:T(8,128)(2,1)}, u32[]{:S(2)}) copy-start(bf16[32,512]{1,0:T(8,128)(2,1)} %param.14) | copy-start | bytes 98308
  5.1 21.3 %collective-permute-start = (bf16[1536,256]{1,0:T(8,128)(2,1)S(1)}, bf16[1536,256]{1,0:T(8,128)(2,1)S(1)}, u32[]{:S(2)}, u32[]{:S(2)}) collective-permute-start(bf16[1536,256]{1,0:T(8,128)(2,1)S(1)} %get-tuple-element.26.refs_0_), channel_id=1, source_target_pairs={{0,8},{8,0},{16,24},{24,16},{1,9},{9,1},{17,25},{25,17},{2,10},{10... | collective-permute-start | bytes 2359304 | tf_op jit(solution)/shard_map/ppermute | solution.py:264
  5.6 20.8 %collective-permute-start.1 = (bf16[1536,256]{1,0:T(8,128)(2,1)S(1)}, bf16[1536,256]{1,0:T(8,128)(2,1)S(1)}, u32[]{:S(2)}, u32[]{:S(2)}) collective-permute-start(bf16[1536,256]{1,0:T(8,128)(2,1)S(1)} %get-tuple-element.27.refs_1_), channel_id=1, source_target_pairs={{0,8},{8,0},{16,24},{24,16},{1,9},{9,1},{17,25},{25,17},{2,10},{10... | collective-permute-start | bytes 2359304 | tf_op jit(solution)/shard_map/ppermute | solution.py:264
  5.7 15.3 %copy-start.3 = (bf16[256,384]{1,0:T(8,128)(2,1)S(1)}, bf16[256,384]{1,0:T(8,128)(2,1)}, u32[]{:S(2)}) copy-start(bf16[256,384]{1,0:T(8,128)(2,1)} %refs_7_.10) | copy-start | bytes 589828
  5.7 20.7 %copy-start.1 = (bf16[384,512]{1,0:T(8,128)(2,1)S(1)}, bf16[384,512]{1,0:T(8,128)(2,1)}, u32[]{:S(2)}) copy-start(bf16[384,512]{1,0:T(8,128)(2,1)} %refs_6_.7) | copy-start | bytes 1179652
  5.7 20.7 %copy-start.2 = (bf16[384,512]{1,0:T(8,128)(2,1)S(1)}, bf16[384,512]{1,0:T(8,128)(2,1)}, u32[]{:S(2)}) copy-start(bf16[384,512]{1,0:T(8,128)(2,1)} %refs_7_.11) | copy-start | bytes 1179652
  5.7 7.6 %collective-permute-start.5 = (bf16[32,1024]{1,0:T(8,128)(2,1)S(1)}, bf16[32,1024]{1,0:T(8,128)(2,1)S(1)}, u32[]{:S(2)}, u32[]{:S(2)}) collective-permute-start(bf16[32,1024]{1,0:T(8,128)(2,1)S(1)} %pad_maximum_fusion.refs_0_), channel_id=1, source_target_pairs={{0,6},{1,7},{2,4},{3,5},{4,2},{5,3},{6,0},{7,1},{8,14},{9,15},{10,... | collective-permute-start | bytes 196616 | tf_op jit(solution)/shard_map/ppermute | solution.py:264
  10.8 5.8 %collective-permute-start.4 = (bf16[32,1024]{1,0:T(8,128)(2,1)S(1)}, bf16[32,1024]{1,0:T(8,128)(2,1)S(1)}, u32[]{:S(2)}, u32[]{:S(2)}) collective-permute-start(bf16[32,1024]{1,0:T(8,128)(2,1)S(1)} %pad_maximum_fusion.refs_0_), channel_id=1, source_target_pairs={{0,4},{1,5},{2,6},{3,7},{4,0},{5,1},{6,2},{7,3},{8,12},{9,13},{10,... | collective-permute-start | bytes 196616 | tf_op jit(solution)/shard_map/ppermute | solution.py:264
  10.8 5.8 %collective-permute-start.3 = (bf16[32,1024]{1,0:T(8,128)(2,1)S(1)}, bf16[32,1024]{1,0:T(8,128)(2,1)S(1)}, u32[]{:S(2)}, u32[]{:S(2)}) collective-permute-start(bf16[32,1024]{1,0:T(8,128)(2,1)S(1)} %pad_maximum_fusion.refs_0_), channel_id=1, source_target_pairs={{0,2},{1,3},{2,0},{3,1},{4,6},{5,7},{6,4},{7,5},{8,10},{9,11},{10,... | collective-permute-start | bytes 196616 | tf_op jit(solution)/shard_map/ppermute | solution.py:264
  16.7 9.2 %collective-permute-start.6 = (bf16[128,1024]{1,0:T(8,128)(2,1)S(1)}, bf16[128,1024]{1,0:T(8,128)(2,1)S(1)}, u32[]{:S(2)}, u32[]{:S(2)}) collective-permute-start(bf16[128,1024]{1,0:T(8,128)(2,1)S(1)} %shard_map.123.refs_8_.refs_5_.refs_6_), channel_id=1, source_target_pairs={{0,1},{1,0},{2,3},{3,2},{4,5},{5,4},{6,7},{7,6},{8,24},{9,25},{10,... | collective-permute-start | bytes 786440 | tf_op jit(solution)/shard_map/ppermute | solution.py:264
  18.2 12.0 %collective-permute-start.7 = (bf16[128,1024]{1,0:T(8,128)(2,1)S(1)}, bf16[128,1024]{1,0:T(8,128)(2,1)S(1)}, u32[]{:S(2)}, u32[]{:S(2)}) collective-permute-start(bf16[128,1024]{1,0:T(8,128)(2,1)S(1)} %shard_map.123.refs_8_.refs_5_.refs_6_), channel_id=1, source_target_pairs={{0,16},{1,17},{2,18},{3,19},{4,20},{5,21},{6,22},{7,23},{8,9},{9,8... | collective-permute-start | bytes 786440 | tf_op jit(solution)/shard_map/ppermute | solution.py:264
  19.7 1.2 %collective-permute-start.2 = (f32[32,128]{1,0:T(8,128)S(1)}, f32[32,128]{1,0:T(8,128)S(1)}, u32[]{:S(2)}, u32[]{:S(2)}) collective-permute-start(f32[32,128]{1,0:T(8,128)S(1)} %get-tuple-element.28.refs_2_), channel_id=1, source_target_pairs={{0,8},{8,0},{16,24},{24,16},{1,9},{9,1},{17,25},{25,17},{2,10},{10... | collective-permute-start | bytes 49160 | tf_op jit(solution)/shard_map/ppermute | solution.py:264
  20.9 9.3 %collective-permute-start.8 = (bf16[256,384]{1,0:T(8,128)(2,1)S(1)}, bf16[256,384]{1,0:T(8,128)(2,1)S(1)}, u32[]{:S(2)}, u32[]{:S(2)}) collective-permute-start(bf16[256,384]{1,0:T(8,128)(2,1)S(1)} %copy-done.3), channel_id=1, source_target_pairs={{0,16},{8,24},{16,0},{24,8},{1,17},{9,25},{17,1},{25,9},{2,18},{10... | collective-permute-start | bytes 589832 | tf_op jit(solution)/shard_map/ppermute | solution.py:264
  25.9 6.5 %collective-permute-start.9 = (bf16[128,1024]{1,0:T(8,128)(2,1)S(1)}, bf16[128,1024]{1,0:T(8,128)(2,1)S(1)}, u32[]{:S(2)}, u32[]{:S(2)}) collective-permute-start(bf16[128,1024]{1,0:T(8,128)(2,1)S(1)} %collective-permute-done.6.refs_8_.refs_6_.refs_7_), channel_id=1, source_target_pairs={{0,16},{1,17},{2,18},{3,19},{4,20},{5,21},{6,22},{7,23},{8,9},{9,8... | collective-permute-start | bytes 786440 | tf_op jit(solution)/shard_map/ppermute | solution.py:264
  33.3 2.6 %collective-permute-start.11 = (bf16[384,256]{1,0:T(8,128)(2,1)S(1)}, bf16[384,256]{1,0:T(8,128)(2,1)S(1)}, u32[]{:S(2)}, u32[]{:S(2)}) collective-permute-start(bf16[384,256]{1,0:T(8,128)(2,1)S(1)} %get-tuple-element.42), channel_id=1, source_target_pairs={{0,8},{8,0},{16,24},{24,16},{1,9},{9,1},{17,25},{25,17},{2,10},{10... | collective-permute-start | bytes 589832 | tf_op jit(solution)/shard_map/ppermute | solution.py:264
  33.4 11.3 %collective-permute-start.14 = (bf16[128,384]{1,0:T(8,128)(2,1)S(1)}, bf16[128,384]{1,0:T(8,128)(2,1)S(1)}, u32[]{:S(2)}, u32[]{:S(2)}) collective-permute-start(bf16[128,384]{1,0:T(8,128)(2,1)S(1)} %get-tuple-element.45), channel_id=1, source_target_pairs={{0,16},{8,24},{16,0},{24,8},{1,17},{9,25},{17,1},{25,9},{2,18},{10... | collective-permute-start | bytes 294920 | tf_op jit(solution)/shard_map/ppermute | solution.py:264
  36.0 3.9 %copy-start = (bf16[384,3072]{1,0:T(8,128)(2,1)S(1)}, bf16[384,3072]{1,0:T(8,128)(2,1)}, u32[]{:S(2)}) copy-start(bf16[384,3072]{1,0:T(8,128)(2,1)} %refs_0_.3) | copy-start | bytes 7077892
  36.0 7.8 %collective-permute-start.12 = (bf16[384,256]{1,0:T(8,128)(2,1)S(1)}, bf16[384,256]{1,0:T(8,128)(2,1)S(1)}, u32[]{:S(2)}, u32[]{:S(2)}) collective-permute-start(bf16[384,256]{1,0:T(8,128)(2,1)S(1)} %add_convert_fusion.1), channel_id=1, source_target_pairs={{0,16},{8,24},{16,0},{24,8},{1,17},{9,25},{17,1},{25,9},{2,18},{10... | collective-permute-start | bytes 589832 | tf_op jit(solution)/shard_map/ppermute | solution.py:264
  38.3 6.9 %collective-permute-start.15 = (bf16[128,384]{1,0:T(8,128)(2,1)S(1)}, bf16[128,384]{1,0:T(8,128)(2,1)S(1)}, u32[]{:S(2)}, u32[]{:S(2)}) collective-permute-start(bf16[128,384]{1,0:T(8,128)(2,1)S(1)} %get-tuple-element.46), channel_id=1, source_target_pairs={{0,16},{8,24},{16,0},{24,8},{1,17},{9,25},{17,1},{25,9},{2,18},{10... | collective-permute-start | bytes 294920 | tf_op jit(solution)/shard_map/ppermute | solution.py:264
  42.4 1.6 %collective-permute-start.10 = (f32[128,384]{1,0:T(8,128)S(1)}, f32[128,384]{1,0:T(8,128)S(1)}, u32[]{:S(2)}, u32[]{:S(2)}) collective-permute-start(f32[128,384]{1,0:T(8,128)S(1)} %get-tuple-element.40), channel_id=1, source_target_pairs={{0,8},{8,0},{16,24},{24,16},{1,9},{9,1},{17,25},{25,17},{2,10},{10... | collective-permute-start | bytes 589832 | tf_op jit(solution)/shard_map/ppermute | solution.py:264
  43.9 1.5 %collective-permute-start.13 = (bf16[384,256]{1,0:T(8,128)(2,1)S(1)}, bf16[384,256]{1,0:T(8,128)(2,1)S(1)}, u32[]{:S(2)}, u32[]{:S(2)}) collective-permute-start(bf16[384,256]{1,0:T(8,128)(2,1)S(1)} %add_convert_fusion.mine_ref), channel_id=1, source_target_pairs={{0,8},{8,0},{16,24},{24,16},{1,9},{9,1},{17,25},{25,17},{2,10},{10... | collective-permute-start | bytes 589832 | tf_op jit(solution)/shard_map/ppermute | solution.py:264

commit v3 on v2

--- a/solution.py
+++ b/solution.py
@@ -111,16 +111,17 @@
 
     blocks = [take(3), take(3)]
     wk_ref, wv_ref, piece = take(3)
-    source = take(2) if mode == "merge" else None
+    source = take({"first": 1, "merge": 2}.get(mode, 0))
     old = take(3) if mode == "merge" else None
     given = take(2) if mode == "rest" else None
     ds_ref = take(1)[0]
-    outs = take({"keep": 2, "merge": 3, "rest": 1}[mode])
+    outs = take({"first": 2, "keep": 2, "merge": 3, "rest": 1}[mode])
     p_ref, dkv_ref, src_ref = refs
     width = wk_ref.shape[1]
     rows = blocks[0][0].shape[0] // HEADS
     stacked = GROUP * rows
     step = 2 * rows
+    size = piece.shape[0]
     if given is not None:
         for x, g in zip(given, (1 - my_core(), my_core())):
             dkv_ref[:, pl.ds(pl.multiple_of(width + g * HEAD_DIM, HEAD_DIM), HEAD_DIM)] = x[...]
@@ -151,21 +152,24 @@
     if mode == "rest":
         outs[0][...] = part.astype(BF16)
         return
+    if mode == "first":
+        outs[0][...] = part
+        pick_source(source[0], None, columns[0], planes, each, src_ref.at[:size, :])
+        outs[1][...] = dot(src_ref[:size, :], dkv_ref[:, width:], TN)
+        return
     if mode == "keep":
         outs[0][...] = part
         outs[1][...] = dkv_ref[:, width:]
         return
-    other_part, *gradients = old
+    other_part, old_total, other_grads = old
     x_ref, y_ref, total_ref = outs
     dx, _ = across(columns[2])
     x_ref[...] = jnp.where(dx == 1, part, other_part[...])
     y_ref[...] = jnp.where(dx == 1, other_part[...], part).astype(BF16)
-    total = None
-    for column, dv_ref in zip(columns, (*gradients, dkv_ref.at[:, width:])):
-        pick_source(*source, column, planes, each, src_ref)
-        term = dot(src_ref[...], dv_ref[...], TN)
-        total = term if total is None else total + term
-    total_ref[...] = total
+    for i in range(2):
+        pick_source(*source, columns[1 + i], planes, each, src_ref.at[i * size : (i + 1) * size, :])
+    both = jnp.concatenate([other_grads[...], dkv_ref[:, width:]], axis=0)
+    total_ref[...] = old_total[...] + dot(src_ref[...], both, TN)
 
 
 def value_kernel(column, planes, each, mine, *refs):
@@ -303,17 +307,18 @@
             [
                 pltpu.VMEM((size, 2 * GROUP * rows), BF16),
                 pltpu.VMEM((size, 2 * width), BF16),
-                pltpu.VMEM((size, cols), BF16),
+                pltpu.VMEM((2 * size, cols), BF16),
             ],
             flops,
             [*targets, w_key, w_value, pieces[c], *extra],
         )
 
     grads = shape((size, width), BF16)
-    ds0, near0, dv0 = chunk(0, "keep", [part_f32, grads], ())
+    wv_shape = shape((cols, width), F32)
+    ds0, near0, total = chunk(0, "first", [part_f32, wv_shape], src[:1])
     ds1, part1, dv1 = chunk(1, "keep", [part_f32, grads], ())
     ds2, near1, far0, total = chunk(
-        2, "merge", [part_f32, part_bf16, shape((cols, width), F32)], (*src, part1, dv0, dv1)
+        2, "merge", [part_f32, part_bf16, wv_shape], (*src, part1, total, dv1)
     )
     y0 = move("y", far0)
     given, sides = [], []

time: 46.7 us -> 49.5 us (1.060)
  waiting for transfers between devices: 13 us -> 16.5 us
  starting transfers between devices: 14.4 us -> 13.8 us
    ppermute x16, waiting for transfers between devices: 13 us -> 16.5 us  [move(): return lax.ppermute(a, axis, pairs)]
    ppermute x16, starting transfers between devices: 14.4 us -> 13.8 us  [move(): return lax.ppermute(a, axis, pairs)]
  transfers between devices with their start and end apart: 16 -> 16, of which waited for: 7 -> 8; matrix products, arithmetic and copies ran while one was open for 2% -> 1% of each run, Pallas kernels for 24% -> 22%
where the time goes in v3:
time: 49.5 us; the launch traced here: 49.2 us
  waiting for transfers between devices  16.5 us (33%)
  starting transfers between devices  13.8 us (28%)
  Pallas kernels  13.2 us (27%)
  local copies, waits for them, and re-layouts  4.12 us (8%)
  between operations  0.84 us (2%)
  other arithmetic  0.76 us (2%)
    ppermute x16, waiting for transfers between devices, move(): return lax.ppermute(a, axis, pairs)  16.5 us
    ppermute x16, starting transfers between devices, move(): return lax.ppermute(a, axis, pairs)  13.8 us
    pallas_call x12, Pallas kernels, call(): pl.pallas_call(kernel, out_shape=outs, in_specs=specs or [VMEM] * len(ope...  13.2 us
    unnamed x20, local copies, waits for them, and re-layouts  4.12 us
  transfers between devices with their start and end apart: 16, of which 8 were waited for; matrix products, arithmetic and copies ran while one was open for 1% of the time, Pallas kernels for 22%

profile of v3, /device:TPU:0, one launch (start us, length us, event | category | flops | bytes accessed | tf_op | source)
XLA Modules:
  0.0 49.2 jit_solution(16475735793919079237)
XLA Ops:
  0.6 1.1 %copy-done.4 = bf16[128,3072]{1,0:T(8,128)(2,1)S(1)} copy-done((bf16[128,3072]{1,0:T(8,128)(2,1)S(1)}, bf16[128,3072]{1,0:T(8,128)(2,1)}, u32[]{:S(2)}) %copy-start.4) | copy-done | bytes 786456
  1.8 1.1 %copy-done.5 = bf16[128,3072]{1,0:T(8,128)(2,1)S(1)} copy-done((bf16[128,3072]{1,0:T(8,128)(2,1)S(1)}, bf16[128,3072]{1,0:T(8,128)(2,1)}, u32[]{:S(2)}) %copy-start.5) | copy-done | bytes 786456
  2.9 1.1 %copy-done.6 = bf16[128,3072]{1,0:T(8,128)(2,1)S(1)} copy-done((bf16[128,3072]{1,0:T(8,128)(2,1)S(1)}, bf16[128,3072]{1,0:T(8,128)(2,1)}, u32[]{:S(2)}) %copy-start.6) | copy-done | bytes 786456
  4.0 0.7 %copy-done.7 = f32[128,12]{0,1:T(8,128)S(1)} copy-done((f32[128,12]{0,1:T(8,128)S(1)}, f32[128,12]{0,1:T(8,128)}, u32[]{:S(2)}) %copy-start.7) | copy-done | bytes 6168
  4.7 0.3 shard_map.121
  5.1 0.5 %collective-permute-start = (bf16[1536,256]{1,0:T(8,128)(2,1)S(1)}, bf16[1536,256]{1,0:T(8,128)(2,1)S(1)}, u32[]{:S(2)}, u32[]{:S(2)}) collective-permute-start(bf16[1536,256]{1,0:T(8,128)(2,1)S(1)} %get-tuple-element.26.refs_0_), channel_id=1, source_target_pairs={{0,8},{8,0},{16,24},{24,16},{1,9},{9,1},{17,25},{25,17},{2,10},{10... | collective-permute-start | bytes 2359304 | tf_op jit(solution)/shard_map/ppermute | solution.py:268
  5.7 3.1 %collective-permute-start.3 = (bf16[32,1024]{1,0:T(8,128)(2,1)S(1)}, bf16[32,1024]{1,0:T(8,128)(2,1)S(1)}, u32[]{:S(2)}, u32[]{:S(2)}) collective-permute-start(bf16[32,1024]{1,0:T(8,128)(2,1)S(1)} %pad_maximum_fusion.refs_0_), channel_id=1, source_target_pairs={{0,2},{1,3},{2,0},{3,1},{4,6},{5,7},{6,4},{7,5},{8,10},{9,11},{10,... | collective-permute-start | bytes 196616 | tf_op jit(solution)/shard_map/ppermute | solution.py:268
  8.8 2.6 %collective-permute-start.4 = (bf16[32,1024]{1,0:T(8,128)(2,1)S(1)}, bf16[32,1024]{1,0:T(8,128)(2,1)S(1)}, u32[]{:S(2)}, u32[]{:S(2)}) collective-permute-start(bf16[32,1024]{1,0:T(8,128)(2,1)S(1)} %pad_maximum_fusion.refs_0_), channel_id=1, source_target_pairs={{0,4},{1,5},{2,6},{3,7},{4,0},{5,1},{6,2},{7,3},{8,12},{9,13},{10,... | collective-permute-start | bytes 196616 | tf_op jit(solution)/shard_map/ppermute | solution.py:268
  11.4 4.9 %collective-permute-done.4.refs_2_ = bf16[32,1024]{1,0:T(8,128)(2,1)S(1)} collective-permute-done((bf16[32,1024]{1,0:T(8,128)(2,1)S(1)}, bf16[32,1024]{1,0:T(8,128)(2,1)S(1)}, u32[]{:S(2)}, u32[]{:S(2)}) %collective-permute-start.4) | collective-permute-done | bytes 65568 | tf_op jit(solution)/shard_map/ppermute | solution.py:268
  16.3 1.3 %collective-permute-done.5.refs_3_ = bf16[32,1024]{1,0:T(8,128)(2,1)S(1)} collective-permute-done((bf16[32,1024]{1,0:T(8,128)(2,1)S(1)}, bf16[32,1024]{1,0:T(8,128)(2,1)S(1)}, u32[]{:S(2)}, u32[]{:S(2)}) %collective-permute-start.5) | collective-permute-done | bytes 65568 | tf_op jit(solution)/shard_map/ppermute | solution.py:268
  17.5 1.6 %collective-permute-start.6 = (bf16[128,1024]{1,0:T(8,128)(2,1)S(1)}, bf16[128,1024]{1,0:T(8,128)(2,1)S(1)}, u32[]{:S(2)}, u32[]{:S(2)}) collective-permute-start(bf16[128,1024]{1,0:T(8,128)(2,1)S(1)} %shard_map.123.refs_8_.refs_5_.refs_6_), channel_id=1, source_target_pairs={{0,1},{1,0},{2,3},{3,2},{4,5},{5,4},{6,7},{7,6},{8,24},{9,25},{10,... | collective-permute-start | bytes 786440 | tf_op jit(solution)/shard_map/ppermute | solution.py:268
  19.1 1.5 %collective-permute-start.7 = (bf16[128,1024]{1,0:T(8,128)(2,1)S(1)}, bf16[128,1024]{1,0:T(8,128)(2,1)S(1)}, u32[]{:S(2)}, u32[]{:S(2)}) collective-permute-start(bf16[128,1024]{1,0:T(8,128)(2,1)S(1)} %shard_map.123.refs_8_.refs_5_.refs_6_), channel_id=1, source_target_pairs={{0,16},{1,17},{2,18},{3,19},{4,20},{5,21},{6,22},{7,23},{8,9},{9,8... | collective-permute-start | bytes 786440 | tf_op jit(solution)/shard_map/ppermute | solution.py:268
  20.6 1.2 %collective-permute-done.2.refs_5_ = f32[32,128]{1,0:T(8,128)S(1)} collective-permute-done((f32[32,128]{1,0:T(8,128)S(1)}, f32[32,128]{1,0:T(8,128)S(1)}, u32[]{:S(2)}, u32[]{:S(2)}) %collective-permute-start.2) | collective-permute-done | bytes 16416 | tf_op jit(solution)/shard_map/ppermute | solution.py:268
  21.8 0.5 %collective-permute-start.8 = (bf16[256,384]{1,0:T(8,128)(2,1)S(1)}, bf16[256,384]{1,0:T(8,128)(2,1)S(1)}, u32[]{:S(2)}, u32[]{:S(2)}) collective-permute-start(bf16[256,384]{1,0:T(8,128)(2,1)S(1)} %copy-done.3), channel_id=1, source_target_pairs={{0,16},{8,24},{16,0},{24,8},{1,17},{9,25},{17,1},{25,9},{2,18},{10... | collective-permute-start | bytes 589832 | tf_op jit(solution)/shard_map/ppermute | solution.py:268
  22.3 3.7 %collective-permute-done.6.refs_8_.refs_6_.refs_7_ = bf16[128,1024]{1,0:T(8,128)(2,1)S(1)} collective-permute-done((bf16[128,1024]{1,0:T(8,128)(2,1)S(1)}, bf16[128,1024]{1,0:T(8,128)(2,1)S(1)}, u32[]{:S(2)}, u32[]{:S(2)}) %collective-permute-start.6) | collective-permute-done | bytes 262176 | tf_op jit(solution)/shard_map/ppermute | solution.py:268
  26.1 2.0 %shard_map.124 = (bf16[128,3072]{1,0:T(8,128)(2,1)S(1)}, f32[128,384]{1,0:T(8,128)S(1)}, f32[384,512]{1,0:T(8,128)S(1)}) custom-call(bf16[1536,256]{1,0:T(8,128)(2,1)S(1)} %get-tuple-element.26.refs_0_, bf16[1536,256]{1,0:T(8,128)(2,1)S(1)} %get-tuple-element.27.refs_1_, f32[32,128]{1,0:T(8,128)S(1)} %get-tuple-element.28.refs_2_, ...), custom_call_target="tpu_custom_call" | custom-call | flops 956301312 | bytes 6193152 | tf_op jit(solution)/shard_map/pallas_call | solution.py:35
  28.1 1.9 %shard_map.125 = (bf16[128,3072]{1,0:T(8,128)(2,1)S(1)}, f32[128,384]{1,0:T(8,128)S(1)}, bf16[128,512]{1,0:T(8,128)(2,1)S(1)}) custom-call(bf16[1536,256]{1,0:T(8,128)(2,1)S(1)} %get-tuple-element.26.refs_0_, bf16[1536,256]{1,0:T(8,128)(2,1)S(1)} %get-tuple-element.27.refs_1_, f32[32,128]{1,0:T(8,128)S(1)} %get-tuple-element.28.refs_2_, ...), custom_call_target="tpu_custom_call" | custom-call | flops 956301312 | bytes 5341184 | tf_op jit(solution)/shard_map/pallas_call | solution.py:35
  30.0 2.0 %shard_map.126 = (bf16[128,3072]{1,0:T(8,128)(2,1)S(1)}, f32[128,384]{1,0:T(8,128)S(1)}, bf16[128,384]{1,0:T(8,128)(2,1)S(1)}, f32[384,512]{1,0:T(8,128)S(1)}) custom-call(bf16[1536,256]{1,0:T(8,128)(2,1)S(1)} %get-tuple-element.26.refs_0_, bf16[1536,256]{1,0:T(8,128)(2,1)S(1)} %get-tuple-element.27.refs_1_, f32[32,128]{1,0:T(8,128)S(1)} %get-tuple-element.28.refs_2_, ...), custom_call_target="tpu_custom_call" | custom-call | flops 956301312 | bytes 7602176 | tf_op jit(solution)/shard_map/pallas_call | solution.py:35
  32.0 0.5 collective-permute-done.9.refs_6_.refs_8_.refs_9_
  32.5 0.9 %shard_map.127 = (bf16[128,256]{1,0:T(8,128)(2,1)S(1)}, bf16[384,256]{1,0:T(8,128)(2,1)S(1)}) custom-call(bf16[1536,256]{1,0:T(8,128)(2,1)S(1)} %get-tuple-element.26.refs_0_, bf16[1536,256]{1,0:T(8,128)(2,1)S(1)} %get-tuple-element.27.refs_1_, f32[32,128]{1,0:T(8,128)S(1)} %get-tuple-element.28.refs_2_, bf16[1536,256]{1,0:T(8,128)(2,1)S(1)} %collective-permute-done.refs_3_, ...), custom_call_target="tpu_custom_call" | custom-call | flops 191260256 | bytes 4882432 | tf_op jit(solution)/shard_map/pallas_call | solution.py:35
  33.5 0.9 %shard_map.128 = (bf16[128,256]{1,0:T(8,128)(2,1)S(1)}, f32[384,256]{1,0:T(8,128)S(1)}) custom-call(bf16[1536,256]{1,0:T(8,128)(2,1)S(1)} %get-tuple-element.26.refs_0_, bf16[1536,256]{1,0:T(8,128)(2,1)S(1)} %get-tuple-element.27.refs_1_, f32[32,128]{1,0:T(8,128)S(1)} %get-tuple-element.28.refs_2_, bf16[1536,256]{1,0:T(8,128)(2,1)S(1)} %collective-permute-done.refs_3_, ...), custom_call_target="tpu_custom_call" | custom-call | flops 191260256 | bytes 5079040 | tf_op jit(solution)/shard_map/pallas_call | solution.py:35
  34.4 0.5 %collective-permute-done.11 = bf16[384,256]{1,0:T(8,128)(2,1)S(1)} collective-permute-done((bf16[384,256]{1,0:T(8,128)(2,1)S(1)}, bf16[384,256]{1,0:T(8,128)(2,1)S(1)}, u32[]{:S(2)}, u32[]{:S(2)}) %collective-permute-start.11) | collective-permute-done | bytes 196640 | tf_op jit(solution)/shard_map/ppermute | solution.py:268
  35.0 1.6 %collective-permute-start.12 = (bf16[384,256]{1,0:T(8,128)(2,1)S(1)}, bf16[384,256]{1,0:T(8,128)(2,1)S(1)}, u32[]{:S(2)}, u32[]{:S(2)}) collective-permute-start(bf16[384,256]{1,0:T(8,128)(2,1)S(1)} %add_convert_fusion.1), channel_id=1, source_target_pairs={{0,16},{8,24},{16,0},{24,8},{1,17},{9,25},{17,1},{25,9},{2,18},{10... | collective-permute-start | bytes 589832 | tf_op jit(solution)/shard_map/ppermute | solution.py:268
  36.6 1.7 %shard_map.129 = (bf16[128,3072]{1,0:T(8,128)(2,1)S(1)}, bf16[128,384]{1,0:T(8,128)(2,1)S(1)}) custom-call(bf16[1536,256]{1,0:T(8,128)(2,1)S(1)} %get-tuple-element.26.refs_0_, bf16[1536,256]{1,0:T(8,128)(2,1)S(1)} %get-tuple-element.27.refs_1_, f32[32,128]{1,0:T(8,128)S(1)} %get-tuple-element.28.refs_2_, ...), custom_call_target="tpu_custom_call" | custom-call | flops 956301312 | bytes 5242880 | tf_op jit(solution)/shard_map/pallas_call | solution.py:35
  38.3 1.2 %shard_map.130.refs_1_ = f32[384,256]{1,0:T(8,128)S(1)} custom-call(bf16[384,3072]{1,0:T(8,128)(2,1)S(1)} %copy-done, bf16[128,3072]{1,0:T(8,128)(2,1)S(1)} %get-tuple-element.29.refs_1_.refs_2_, bf16[128,3072]{1,0:T(8,128)(2,1)S(1)} %get-tuple-element.30.refs_2_.refs_3_, bf16[128,3072]{1,0:T(8,128)(2,1)S(1)} %get-tuple-element.34.refs_3_.refs_4_, ...), custom_call_target="tpu_custom_call" | custom-call | flops 704643072 | bytes 6946816 | tf_op jit(solution)/shard_map/pallas_call | solution.py:35
  39.5 1.3 %shard_map.131 = (f32[128,384]{1,0:T(8,128)S(1)}, f32[128,384]{1,0:T(8,128)S(1)}) custom-call(bf16[384,3072]{1,0:T(8,128)(2,1)S(1)} %copy-done, f32[384,256]{1,0:T(8,128)S(1)} %shard_map.130.refs_1_, bf16[128,3072]{1,0:T(8,128)(2,1)S(1)} %get-tuple-element.29.refs_1_.refs_2_, bf16[128,3072]{1,0:T(8,128)(2,1)S(1)} %get-tuple-element.30.refs_2_.refs_3_, ...), custom_call_target="tpu_custom_call" | custom-call | flops 704643072 | bytes 7340032 | tf_op jit(solution)/shard_map/pallas_call | solution.py:35
  40.9 0.5 %collective-permute-start.14 = (bf16[128,384]{1,0:T(8,128)(2,1)S(1)}, bf16[128,384]{1,0:T(8,128)(2,1)S(1)}, u32[]{:S(2)}, u32[]{:S(2)}) collective-permute-start(bf16[128,384]{1,0:T(8,128)(2,1)S(1)} %get-tuple-element.45), channel_id=1, source_target_pairs={{0,16},{8,24},{16,0},{24,8},{1,17},{9,25},{17,1},{25,9},{2,18},{10... | collective-permute-start | bytes 294920 | tf_op jit(solution)/shard_map/ppermute | solution.py:268
  41.4 1.5 %collective-permute-start.15 = (bf16[128,384]{1,0:T(8,128)(2,1)S(1)}, bf16[128,384]{1,0:T(8,128)(2,1)S(1)}, u32[]{:S(2)}, u32[]{:S(2)}) collective-permute-start(bf16[128,384]{1,0:T(8,128)(2,1)S(1)} %get-tuple-element.46), channel_id=1, source_target_pairs={{0,16},{8,24},{16,0},{24,8},{1,17},{9,25},{17,1},{25,9},{2,18},{10... | collective-permute-start | bytes 294920 | tf_op jit(solution)/shard_map/ppermute | solution.py:268
  43.1 0.7 %add_convert_fusion.2 = bf16[128,384]{1,0:T(8,128)(2,1)} fusion(f32[128,384]{1,0:T(8,128)S(1)} %get-tuple-element.39, f32[128,384]{1,0:T(8,128)S(1)} %collective-permute-done.10), kind=kLoop, calls=%fused_computation.2 | loop fusion | flops 98304 | bytes 491520 | tf_op jit(solution)/shard_map/convert_element_type | solution.py:359
  43.8 2.8 %collective-permute-done.14.y0_ref = bf16[128,384]{1,0:T(8,128)(2,1)S(1)} collective-permute-done((bf16[128,384]{1,0:T(8,128)(2,1)S(1)}, bf16[128,384]{1,0:T(8,128)(2,1)S(1)}, u32[]{:S(2)}, u32[]{:S(2)}) %collective-permute-start.14) | collective-permute-done | bytes 98336 | tf_op jit(solution)/shard_map/ppermute | solution.py:268
  46.6 1.6 %collective-permute-done.15.y1_ref = bf16[128,384]{1,0:T(8,128)(2,1)S(1)} collective-permute-done((bf16[128,384]{1,0:T(8,128)(2,1)S(1)}, bf16[128,384]{1,0:T(8,128)(2,1)S(1)}, u32[]{:S(2)}, u32[]{:S(2)}) %collective-permute-start.15) | collective-permute-done | bytes 98336 | tf_op jit(solution)/shard_map/ppermute | solution.py:268
  48.2 1.0 %shard_map.132 = (bf16[256,384]{1,0:T(8,128)(2,1)}, f32[384,512]{1,0:T(8,128)}) custom-call(bf16[384,256]{1,0:T(8,128)(2,1)S(1)} %add_convert_fusion.mine_ref, bf16[384,256]{1,0:T(8,128)(2,1)S(1)} %collective-permute-done.13.other_ref, f32[128,384]{1,0:T(8,128)S(1)} %get-tuple-element.43.near0_ref, f32[128,384]{1,0:T(8,128)S(1)} %get-tuple-element.44.near1_ref, ...), custom_call_target="tpu_custom_call" | custom-call | flops 196608 | bytes 1966080 | tf_op jit(solution)/shard_map/pallas_call | solution.py:35
  (36 shorter events, 0.5 us)
Async XLA Ops:
  0.6 1.1 %copy-start.4 = (bf16[128,3072]{1,0:T(8,128)(2,1)S(1)}, bf16[128,3072]{1,0:T(8,128)(2,1)}, u32[]{:S(2)}) copy-start(bf16[128,3072]{1,0:T(8,128)(2,1)} %q_ref.1) | copy-start | bytes 2359300
  1.8 1.1 %copy-start.5 = (bf16[128,3072]{1,0:T(8,128)(2,1)S(1)}, bf16[128,3072]{1,0:T(8,128)(2,1)}, u32[]{:S(2)}) copy-start(bf16[128,3072]{1,0:T(8,128)(2,1)} %do_ref.1) | copy-start | bytes 2359300
  2.9 1.1 %copy-start.6 = (bf16[128,3072]{1,0:T(8,128)(2,1)S(1)}, bf16[128,3072]{1,0:T(8,128)(2,1)}, u32[]{:S(2)}) copy-start(bf16[128,3072]{1,0:T(8,128)(2,1)} %o_ref.1) | copy-start | bytes 2359300
  4.0 0.7 %copy-start.7 = (f32[128,12]{0,1:T(8,128)S(1)}, f32[128,12]{0,1:T(8,128)}, u32[]{:S(2)}) copy-start(f32[128,12]{0,1:T(8,128)} %param.12) | copy-start | bytes 18436
  4.7 0.9 %copy-start.8 = (bf16[32,512]{1,0:T(8,128)(2,1)S(1)}, bf16[32,512]{1,0:T(8,128)(2,1)}, u32[]{:S(2)}) copy-start(bf16[32,512]{1,0:T(8,128)(2,1)} %param.15) | copy-start | bytes 98308
  4.7 0.9 %copy-start.9 = (bf16[32,512]{1,0:T(8,128)(2,1)S(1)}, bf16[32,512]{1,0:T(8,128)(2,1)}, u32[]{:S(2)}) copy-start(bf16[32,512]{1,0:T(8,128)(2,1)} %param.14) | copy-start | bytes 98308
  5.1 21.0 %collective-permute-start = (bf16[1536,256]{1,0:T(8,128)(2,1)S(1)}, bf16[1536,256]{1,0:T(8,128)(2,1)S(1)}, u32[]{:S(2)}, u32[]{:S(2)}) collective-permute-start(bf16[1536,256]{1,0:T(8,128)(2,1)S(1)} %get-tuple-element.26.refs_0_), channel_id=1, source_target_pairs={{0,8},{8,0},{16,24},{24,16},{1,9},{9,1},{17,25},{25,17},{2,10},{10... | collective-permute-start | bytes 2359304 | tf_op jit(solution)/shard_map/ppermute | solution.py:268
  5.6 20.5 %collective-permute-start.1 = (bf16[1536,256]{1,0:T(8,128)(2,1)S(1)}, bf16[1536,256]{1,0:T(8,128)(2,1)S(1)}, u32[]{:S(2)}, u32[]{:S(2)}) collective-permute-start(bf16[1536,256]{1,0:T(8,128)(2,1)S(1)} %get-tuple-element.27.refs_1_), channel_id=1, source_target_pairs={{0,8},{8,0},{16,24},{24,16},{1,9},{9,1},{17,25},{25,17},{2,10},{10... | collective-permute-start | bytes 2359304 | tf_op jit(solution)/shard_map/ppermute | solution.py:268
  5.7 16.1 %copy-start.3 = (bf16[256,384]{1,0:T(8,128)(2,1)S(1)}, bf16[256,384]{1,0:T(8,128)(2,1)}, u32[]{:S(2)}) copy-start(bf16[256,384]{1,0:T(8,128)(2,1)} %refs_7_.10) | copy-start | bytes 589828
  5.7 20.4 %copy-start.1 = (bf16[384,512]{1,0:T(8,128)(2,1)S(1)}, bf16[384,512]{1,0:T(8,128)(2,1)}, u32[]{:S(2)}) copy-start(bf16[384,512]{1,0:T(8,128)(2,1)} %refs_6_.7) | copy-start | bytes 1179652
  5.7 20.4 %copy-start.2 = (bf16[384,512]{1,0:T(8,128)(2,1)S(1)}, bf16[384,512]{1,0:T(8,128)(2,1)}, u32[]{:S(2)}) copy-start(bf16[384,512]{1,0:T(8,128)(2,1)} %refs_7_.11) | copy-start | bytes 1179652
  5.7 5.7 %collective-permute-start.3 = (bf16[32,1024]{1,0:T(8,128)(2,1)S(1)}, bf16[32,1024]{1,0:T(8,128)(2,1)S(1)}, u32[]{:S(2)}, u32[]{:S(2)}) collective-permute-start(bf16[32,1024]{1,0:T(8,128)(2,1)S(1)} %pad_maximum_fusion.refs_0_), channel_id=1, source_target_pairs={{0,2},{1,3},{2,0},{3,1},{4,6},{5,7},{6,4},{7,5},{8,10},{9,11},{10,... | collective-permute-start | bytes 196616 | tf_op jit(solution)/shard_map/ppermute | solution.py:268
  8.8 7.5 %collective-permute-start.4 = (bf16[32,1024]{1,0:T(8,128)(2,1)S(1)}, bf16[32,1024]{1,0:T(8,128)(2,1)S(1)}, u32[]{:S(2)}, u32[]{:S(2)}) collective-permute-start(bf16[32,1024]{1,0:T(8,128)(2,1)S(1)} %pad_maximum_fusion.refs_0_), channel_id=1, source_target_pairs={{0,4},{1,5},{2,6},{3,7},{4,0},{5,1},{6,2},{7,3},{8,12},{9,13},{10,... | collective-permute-start | bytes 196616 | tf_op jit(solution)/shard_map/ppermute | solution.py:268
  11.4 6.2 %collective-permute-start.5 = (bf16[32,1024]{1,0:T(8,128)(2,1)S(1)}, bf16[32,1024]{1,0:T(8,128)(2,1)S(1)}, u32[]{:S(2)}, u32[]{:S(2)}) collective-permute-start(bf16[32,1024]{1,0:T(8,128)(2,1)S(1)} %pad_maximum_fusion.refs_0_), channel_id=1, source_target_pairs={{0,6},{1,7},{2,4},{3,5},{4,2},{5,3},{6,0},{7,1},{8,14},{9,15},{10,... | collective-permute-start | bytes 196616 | tf_op jit(solution)/shard_map/ppermute | solution.py:268
  17.5 8.5 %collective-permute-start.6 = (bf16[128,1024]{1,0:T(8,128)(2,1)S(1)}, bf16[128,1024]{1,0:T(8,128)(2,1)S(1)}, u32[]{:S(2)}, u32[]{:S(2)}) collective-permute-start(bf16[128,1024]{1,0:T(8,128)(2,1)S(1)} %shard_map.123.refs_8_.refs_5_.refs_6_), channel_id=1, source_target_pairs={{0,1},{1,0},{2,3},{3,2},{4,5},{5,4},{6,7},{7,6},{8,24},{9,25},{10,... | collective-permute-start | bytes 786440 | tf_op jit(solution)/shard_map/ppermute | solution.py:268
  19.1 10.9 %collective-permute-start.7 = (bf16[128,1024]{1,0:T(8,128)(2,1)S(1)}, bf16[128,1024]{1,0:T(8,128)(2,1)S(1)}, u32[]{:S(2)}, u32[]{:S(2)}) collective-permute-start(bf16[128,1024]{1,0:T(8,128)(2,1)S(1)} %shard_map.123.refs_8_.refs_5_.refs_6_), channel_id=1, source_target_pairs={{0,16},{1,17},{2,18},{3,19},{4,20},{5,21},{6,22},{7,23},{8,9},{9,8... | collective-permute-start | bytes 786440 | tf_op jit(solution)/shard_map/ppermute | solution.py:268
  20.6 1.2 %collective-permute-start.2 = (f32[32,128]{1,0:T(8,128)S(1)}, f32[32,128]{1,0:T(8,128)S(1)}, u32[]{:S(2)}, u32[]{:S(2)}) collective-permute-start(f32[32,128]{1,0:T(8,128)S(1)} %get-tuple-element.28.refs_2_), channel_id=1, source_target_pairs={{0,8},{8,0},{16,24},{24,16},{1,9},{9,1},{17,25},{25,17},{2,10},{10... | collective-permute-start | bytes 49160 | tf_op jit(solution)/shard_map/ppermute | solution.py:268
  21.8 8.2 %collective-permute-start.8 = (bf16[256,384]{1,0:T(8,128)(2,1)S(1)}, bf16[256,384]{1,0:T(8,128)(2,1)S(1)}, u32[]{:S(2)}, u32[]{:S(2)}) collective-permute-start(bf16[256,384]{1,0:T(8,128)(2,1)S(1)} %copy-done.3), channel_id=1, source_target_pairs={{0,16},{8,24},{16,0},{24,8},{1,17},{9,25},{17,1},{25,9},{2,18},{10... | collective-permute-start | bytes 589832 | tf_op jit(solution)/shard_map/ppermute | solution.py:268
  26.1 6.4 %collective-permute-start.9 = (bf16[128,1024]{1,0:T(8,128)(2,1)S(1)}, bf16[128,1024]{1,0:T(8,128)(2,1)S(1)}, u32[]{:S(2)}, u32[]{:S(2)}) collective-permute-start(bf16[128,1024]{1,0:T(8,128)(2,1)S(1)} %collective-permute-done.6.refs_8_.refs_6_.refs_7_), channel_id=1, source_target_pairs={{0,16},{1,17},{2,18},{3,19},{4,20},{5,21},{6,22},{7,23},{8,9},{9,8... | collective-permute-start | bytes 786440 | tf_op jit(solution)/shard_map/ppermute | solution.py:268
  33.4 1.5 %collective-permute-start.11 = (bf16[384,256]{1,0:T(8,128)(2,1)S(1)}, bf16[384,256]{1,0:T(8,128)(2,1)S(1)}, u32[]{:S(2)}, u32[]{:S(2)}) collective-permute-start(bf16[384,256]{1,0:T(8,128)(2,1)S(1)} %get-tuple-element.42), channel_id=1, source_target_pairs={{0,8},{8,0},{16,24},{24,16},{1,9},{9,1},{17,25},{25,17},{2,10},{10... | collective-permute-start | bytes 589832 | tf_op jit(solution)/shard_map/ppermute | solution.py:268
  34.9 3.4 %copy-start = (bf16[384,3072]{1,0:T(8,128)(2,1)S(1)}, bf16[384,3072]{1,0:T(8,128)(2,1)}, u32[]{:S(2)}) copy-start(bf16[384,3072]{1,0:T(8,128)(2,1)} %refs_0_.3) | copy-start | bytes 7077892
  35.0 8.0 %collective-permute-start.12 = (bf16[384,256]{1,0:T(8,128)(2,1)S(1)}, bf16[384,256]{1,0:T(8,128)(2,1)S(1)}, u32[]{:S(2)}, u32[]{:S(2)}) collective-permute-start(bf16[384,256]{1,0:T(8,128)(2,1)S(1)} %add_convert_fusion.1), channel_id=1, source_target_pairs={{0,16},{8,24},{16,0},{24,8},{1,17},{9,25},{17,1},{25,9},{2,18},{10... | collective-permute-start | bytes 589832 | tf_op jit(solution)/shard_map/ppermute | solution.py:268
  40.8 2.3 %collective-permute-start.10 = (f32[128,384]{1,0:T(8,128)S(1)}, f32[128,384]{1,0:T(8,128)S(1)}, u32[]{:S(2)}, u32[]{:S(2)}) collective-permute-start(f32[128,384]{1,0:T(8,128)S(1)} %get-tuple-element.40), channel_id=1, source_target_pairs={{0,8},{8,0},{16,24},{24,16},{1,9},{9,1},{17,25},{25,17},{2,10},{10... | collective-permute-start | bytes 589832 | tf_op jit(solution)/shard_map/ppermute | solution.py:268
  40.9 5.7 %collective-permute-start.14 = (bf16[128,384]{1,0:T(8,128)(2,1)S(1)}, bf16[128,384]{1,0:T(8,128)(2,1)S(1)}, u32[]{:S(2)}, u32[]{:S(2)}) collective-permute-start(bf16[128,384]{1,0:T(8,128)(2,1)S(1)} %get-tuple-element.45), channel_id=1, source_target_pairs={{0,16},{8,24},{16,0},{24,8},{1,17},{9,25},{17,1},{25,9},{2,18},{10... | collective-permute-start | bytes 294920 | tf_op jit(solution)/shard_map/ppermute | solution.py:268
  41.4 6.8 %collective-permute-start.15 = (bf16[128,384]{1,0:T(8,128)(2,1)S(1)}, bf16[128,384]{1,0:T(8,128)(2,1)S(1)}, u32[]{:S(2)}, u32[]{:S(2)}) collective-permute-start(bf16[128,384]{1,0:T(8,128)(2,1)S(1)} %get-tuple-element.46), channel_id=1, source_target_pairs={{0,16},{8,24},{16,0},{24,8},{1,17},{9,25},{17,1},{25,9},{2,18},{10... | collective-permute-start | bytes 294920 | tf_op jit(solution)/shard_map/ppermute | solution.py:268
  43.0 5.2 %collective-permute-start.13 = (bf16[384,256]{1,0:T(8,128)(2,1)S(1)}, bf16[384,256]{1,0:T(8,128)(2,1)S(1)}, u32[]{:S(2)}, u32[]{:S(2)}) collective-permute-start(bf16[384,256]{1,0:T(8,128)(2,1)S(1)} %add_convert_fusion.mine_ref), channel_id=1, source_target_pairs={{0,8},{8,0},{16,24},{24,16},{1,9},{9,1},{17,25},{25,17},{2,10},{10... | collective-permute-start | bytes 589832 | tf_op jit(solution)/shard_map/ppermute | solution.py:268
